TPU v7x, 256 devices: a whole 4x4x8 slice. The times are simulated.
256 devices in a mesh: sp: 16 (over y, x), tp: 16 (over z, core).
Axes of the slice: x: 4, y: 4, z: 8, core: 2. Of those that a mesh axis runs over, the one named last changes fastest.
Arguments:
- moe_input: bfloat16 [2048, 2048], P('sp'), may hold values from -6 to 6
- cotangent: bfloat16 [2048, 2048], P('sp'), may hold values from -6 to 6
- route_expert: int32 [2048, 2], P('sp'), may hold values from 0 to 15, all different within a row; in each aligned block of 128 rows (0 to 127, 128 to 255, ...) at most 32 rows name the same one
- route_weight: float32 [2048, 2], P('sp'), may hold values from 0.2 to 1
- w_gate: bfloat16 [16, 2048, 6144], P('sp', None, 'tp'), may hold values from -0.125 to 0.125
- w_up: bfloat16 [16, 2048, 6144], P('sp', None, 'tp'), may hold values from -0.125 to 0.125
- w_down: bfloat16 [16, 6144, 2048], P('sp', 'tp'), may hold values from -0.078125 to 0.078125
- out_proj: bfloat16 [2048, 2048], P('tp'), may hold values from -0.125 to 0.125
- saved_out: bfloat16 [2048, 2048], P('sp', 'tp'), may hold values from -6 to 6
- queries: bfloat16 [2048, 1024], P('sp', 'tp'), may hold values from -6 to 6
- keys: bfloat16 [2048, 1024], P('sp', 'tp'), may hold values from -6 to 6
- values: bfloat16 [2048, 2048], P('sp', 'tp'), may hold values from -6 to 6
- log_decay: float32 [2048, 1024], P('sp', 'tp'), may hold values from -1 to 0
- span_state: float32 [32, 1024, 128], P('sp', 'tp'), may hold values from -6 to 6
Outputs:
- grad_w_gate: bfloat16 [16, 2048, 6144], P('sp', None, 'tp')
- grad_w_up: bfloat16 [16, 2048, 6144], P('sp', None, 'tp')
- grad_w_down: bfloat16 [16, 6144, 2048], P('sp', 'tp')
- grad_proj: float32 [2048, 2048], P('sp', 'tp')
- grad_queries: bfloat16 [2048, 1024], P('sp', 'tp')
- grad_keys: bfloat16 [2048, 1024], P('sp', 'tp')
- grad_values: bfloat16 [2048, 2048], P('sp', 'tp')
- grad_decay: float32 [2048, 1024], P('sp', 'tp')
Inputs may be any that keep to these rules, and one draw needn't show every extreme that they name: `route_expert`: each row names two different experts. Within the 128 rows of one index of sp no expert is named by more than 32 rows, a bound that some block reaches.
All inputs are finite; a program needn't handle non-finite values.
Results may differ from a plain program's by a relative error of at most 0.019.
Values may be sent and summed in bfloat16 or wider, within the bound.
A program may use at most 128 MiB of HBM per device.

v0:
```python
import jax
import jax.numpy as jnp
from jax import lax
from jax.sharding import PartitionSpec as P

DK = 64
SPAN = 64


def in_one_piece(arrays, axis, split_dim, concat_dim, along):
    widths = [a.shape[along] for a in arrays]
    both = jnp.concatenate(arrays, axis=along)
    filled = lax.all_to_all(both, axis, split_axis=split_dim, concat_axis=concat_dim, tiled=True)
    return tuple(jnp.split(filled, [sum(widths[:k]) for k in range(1, len(widths))], axis=along))


def over_pieces(shard, axis):
    parts = lax.all_gather(shard, axis).astype(jnp.float32)
    return parts.sum(axis=0)


def in_blocks(shard, dim, length):
    shape = shard.shape
    parts = shard.reshape(*shape[:dim], length, shape[dim] // length, *shape[dim + 1 :])
    return jnp.moveaxis(parts, dim, 0)


def sum_at_owner(shard, axis, dim):
    parts = in_blocks(shard, dim, lax.axis_size(axis))
    arrived = lax.all_to_all(parts, axis, split_axis=0, concat_axis=0, tiled=True)
    return arrived.astype(jnp.float32).sum(axis=0)


def copy_for_each(shard, axis):
    length = lax.axis_size(axis)
    return lax.all_to_all(
        jnp.broadcast_to(shard[None], (length, *shard.shape)), axis, 0, 0, tiled=True
    )


def all_in_one(shard, axis):
    leaves = jax.tree.leaves(shard)
    sequence = sorted(range(len(leaves)), key=lambda k: -leaves[k].size)
    width = (1, *leaves[sequence[0]].shape)[-1]
    lines = [
        jnp.pad(leaves[k].reshape(-1), (0, -leaves[k].size % width)).reshape(-1, width)
        for k in sequence
    ]
    both, at, found = (copy_for_each(jnp.concatenate(lines), axis), 0, {})
    for k, line in zip(sequence, lines):
        slab = both[:, at : at + len(line)].reshape(len(both), -1)
        found[k] = slab[:, : leaves[k].size].reshape(-1, *leaves[k].shape)
        at += len(line)
    numbers = iter(range(len(leaves)))
    return jax.tree.map(lambda _: found[next(numbers)], shard)


def combined_pairwise(pieces, combine):
    while len(jax.tree.leaves(pieces)[0]) > 1:
        pieces = jax.vmap(combine)(
            *(jax.tree.map(lambda part: part[side::2], pieces) for side in (0, 1))
        )
    return jax.tree.map(lambda part: part[0], pieces)


def carried_in(shard, axis, combine, identity):
    length, mine = (lax.axis_size(axis), lax.axis_index(axis))
    passed = jnp.arange(length) > mine

    def kept(part, zero, own):
        part = jnp.where(
            passed.reshape(-1, *(1 for _ in own.shape)), part, jnp.asarray(zero, own.dtype)
        )
        return part[::-1]

    pieces = all_in_one(shard, axis)
    return combined_pairwise(jax.tree.map(kept, pieces, identity, shard), combine)


def slot_places(experts, count):
    routes_flat = experts.reshape(-1)
    one_hot = (routes_flat[:, None] == jnp.arange(count, dtype=jnp.int32)[None, :]).astype(
        jnp.int32
    )
    earlier = jnp.cumsum(one_hot, axis=0) - one_hot
    return jnp.sum(earlier * one_hot, axis=1).reshape(experts.shape)


def expert_grads(inputs, routed, gate_weight, up_weight, down_weight):
    gate = jnp.dot(inputs, gate_weight, preferred_element_type=jnp.float32)
    upper = jnp.dot(inputs, up_weight, preferred_element_type=jnp.float32)
    sigmoid_gate = jax.nn.sigmoid(gate)
    active = gate * sigmoid_gate
    hidden = (active * upper).astype(jnp.bfloat16)
    d_hidden = lax.dot_general(
        routed, down_weight, (((1,), (1,)), ((), ())), preferred_element_type=jnp.float32
    )
    d_upper = (d_hidden * active).astype(jnp.bfloat16)
    d_gate = (d_hidden * upper * sigmoid_gate * (1.0 + gate * (1.0 - sigmoid_gate))).astype(
        jnp.bfloat16
    )
    grad_down = lax.dot_general(
        hidden, routed, (((0,), (0,)), ((), ())), preferred_element_type=jnp.float32
    ).astype(jnp.bfloat16)
    grad_gate = lax.dot_general(
        inputs, d_gate, (((0,), (0,)), ((), ())), preferred_element_type=jnp.float32
    ).astype(jnp.bfloat16)
    grad_up = lax.dot_general(
        inputs, d_upper, (((0,), (0,)), ((), ())), preferred_element_type=jnp.float32
    ).astype(jnp.bfloat16)
    return (d_gate, d_upper, grad_gate, grad_up, grad_down)


def input_grad(d_gate, d_upper, gate_weight, up_weight):
    first = lax.dot_general(
        d_gate, gate_weight, (((1,), (1,)), ((), ())), preferred_element_type=jnp.float32
    )
    second = lax.dot_general(
        d_upper, up_weight, (((1,), (1,)), ((), ())), preferred_element_type=jnp.float32
    )
    return first + second


def gated_pieces(queries, keys, values, log_decay, grad_mix, key_dim, span_len):
    value_dim = values.shape[1] * key_dim // queries.shape[1]
    heads = queries.shape[1] // key_dim
    spans = queries.shape[0] // span_len

    def blocks(array, width):
        return array.astype(jnp.float32).reshape(spans, span_len, heads, width)

    query_spans = blocks(queries, key_dim)
    key_spans = blocks(keys, key_dim)
    value_spans = blocks(values, value_dim)
    grad_spans = blocks(grad_mix, value_dim)
    cumulative = jnp.cumsum(blocks(log_decay, key_dim), axis=1)
    last = cumulative[:, -1]
    scale = key_dim ** (-0.5)
    query_decayed = query_spans * jnp.exp(cumulative)
    key_grown = key_spans * jnp.exp(-cumulative)
    key_to_end = key_spans * jnp.exp(last[:, None] - cumulative)
    g_local = scale * jnp.einsum("nthk,nthv->nhkv", query_decayed, grad_spans)
    return (
        query_spans,
        key_spans,
        value_spans,
        grad_spans,
        cumulative,
        last,
        query_decayed,
        key_grown,
        key_to_end,
        g_local,
    )


def backward_step(carry, inputs):
    local, decay = inputs
    return (local + jnp.exp(decay)[..., None] * carry, carry)


def gated_finish(pieces, span_state, g_end, key_dim):
    (
        query_spans,
        key_spans,
        value_spans,
        grad_spans,
        cumulative,
        last,
        query_decayed,
        key_grown,
        key_to_end,
        g_local,
    ) = pieces
    spans, span_len, heads, value_dim = value_spans.shape
    scale = key_dim ** (-0.5)
    token_locations = jnp.arange(span_len, dtype=jnp.int32)
    causal = (token_locations[:, None] >= token_locations[None, :]).astype(jnp.float32)
    scores = jnp.einsum("nthk,nshk->nhts", query_decayed, key_grown) * causal
    grad_dot = jnp.einsum("nthv,nshv->nhts", grad_spans, value_spans) * causal
    state = span_state.reshape(spans, heads, key_dim, value_dim)
    d_query = (
        scale
        * jnp.exp(cumulative)
        * (
            jnp.einsum("nhts,nshk->nthk", grad_dot, key_grown)
            + jnp.einsum("nthv,nhkv->nthk", grad_spans, state)
        )
    )
    d_key = scale * jnp.exp(-cumulative) * jnp.einsum(
        "nhts,nthk->nshk", grad_dot, query_decayed
    ) + jnp.exp(last[:, None] - cumulative) * jnp.einsum("nshv,nhkv->nshk", value_spans, g_end)
    d_value = scale * jnp.einsum("nhts,nthv->nshv", scores, grad_spans) + jnp.einsum(
        "nshk,nhkv->nshv", key_to_end, g_end
    )
    state_end = jnp.exp(last)[..., None] * state + jnp.einsum(
        "nshk,nshv->nhkv", key_to_end, value_spans
    )
    tail = jnp.sum(state_end * g_end, axis=-1)
    d_cumulative = query_spans * d_query - key_spans * d_key
    d_log = jnp.cumsum(d_cumulative[:, ::-1], axis=1)[:, ::-1] + tail[:, None]
    rows = spans * span_len
    return (
        d_query.reshape(rows, heads * key_dim).astype(jnp.bfloat16),
        d_key.reshape(rows, heads * key_dim).astype(jnp.bfloat16),
        d_value.reshape(rows, heads * value_dim).astype(jnp.bfloat16),
        d_log.reshape(rows, heads * key_dim),
    )


def carry_combine(earlier, later):
    return (later[0] * earlier[0], later[1] + later[0][..., None] * earlier[1])


def on_device(
    moe_input,
    cotangent,
    route_expert,
    route_weight,
    w_gate,
    w_up,
    w_down,
    out_proj,
    saved_out,
    queries,
    keys,
    values,
    log_decay,
    span_state,
):
    tok_rows, width = moe_input.shape
    groups = lax.axis_size("sp")
    capacity = 4 * tok_rows // groups
    target_locations = slot_places(route_expert, groups)
    rows_index = (target_locations * groups + route_expert).reshape(-1)
    owner = (
        jnp.full((capacity * groups,), 2 * tok_rows, jnp.int32)
        .at[rows_index]
        .set(jnp.arange(2 * tok_rows, dtype=jnp.int32))
    )
    weighted = (route_weight[:, :, None] * cotangent[:, None, :].astype(jnp.float32)).astype(
        jnp.bfloat16
    )
    weighted = weighted.reshape(2 * tok_rows, width)
    blank = jnp.zeros((1, width), jnp.bfloat16)
    send_in = jnp.concatenate([moe_input, blank], axis=0)[owner // 2].reshape(
        capacity, groups, width
    )
    send_cot = jnp.concatenate([weighted, blank], axis=0)[owner].reshape(capacity, groups, width)
    gate_weight = w_gate[0]
    up_weight = w_up[0]
    down_weight = w_down[0]
    got_in, got_cot = in_one_piece((send_in, send_cot), "sp", 1, 1, 0)
    d_gate, d_upper, grad_gate, grad_up, grad_down = expert_grads(
        got_in.reshape(-1, width), got_cot.reshape(-1, width), gate_weight, up_weight, down_weight
    )
    partial_value = input_grad(d_gate, d_upper, gate_weight, up_weight).reshape(
        capacity, groups, width
    )
    returned = (
        lax.all_to_all(
            partial_value.astype(jnp.bfloat16), "sp", split_axis=1, concat_axis=1, tiled=True
        )
        .astype(partial_value.dtype)
        .reshape(-1, width)
    )
    picked = returned[rows_index]
    routed = jnp.sum(picked.reshape(tok_rows, 2, width), axis=1)
    total = over_pieces(routed.astype(jnp.bfloat16), "tp").astype(jnp.float32)
    grad_in = (cotangent.astype(jnp.float32) + total).astype(jnp.bfloat16)
    grad_mix = lax.dot_general(
        grad_in, out_proj, (((1,), (1,)), ((), ())), preferred_element_type=jnp.float32
    )
    grad_proj = sum_at_owner(
        lax.dot_general(
            grad_in, saved_out, (((0,), (0,)), ((), ())), preferred_element_type=jnp.float32
        ).astype(jnp.bfloat16),
        "sp",
        0,
    )
    pieces = gated_pieces(queries, keys, values, log_decay, grad_mix, DK, SPAN)
    g_local = pieces[9]
    last = pieces[5]
    begin = jnp.zeros(g_local.shape[1:], jnp.float32)
    device_start, local_end = lax.scan(backward_step, begin, (g_local, last), reverse=True)
    device_decay = jnp.exp(jnp.sum(last, axis=0))
    identity = (jnp.ones_like(device_decay), jnp.zeros_like(device_start))
    decay_after, state_after = carried_in(
        (device_decay, device_start), "sp", carry_combine, identity
    )
    running = jnp.cumsum(last, axis=0)
    beyond = running[-1][None] - running
    g_end = local_end + jnp.exp(beyond)[..., None] * state_after[None]
    grad_queries, grad_keys, grad_values, grad_decay = gated_finish(pieces, span_state, g_end, DK)
    return (
        grad_gate[None],
        grad_up[None],
        grad_down[None],
        grad_proj,
        grad_queries,
        grad_keys,
        grad_values,
        grad_decay,
    )


def solution(mesh):
    placed = (
        P("sp", None),
        P("sp", None),
        P("sp", None),
        P("sp", None),
        P("sp", None, "tp"),
        P("sp", None, "tp"),
        P("sp", "tp", None),
        P("tp", None),
        P("sp", "tp"),
        P("sp", "tp"),
        P("sp", "tp"),
        P("sp", "tp"),
        P("sp", "tp"),
        P("sp", "tp", None),
    )
    return jax.shard_map(
        on_device,
        mesh=mesh,
        in_specs=placed,
        out_specs=(
            P("sp", None, "tp"),
            P("sp", None, "tp"),
            P("sp", "tp", None),
            P("sp", "tp"),
            P("sp", "tp"),
            P("sp", "tp"),
            P("sp", "tp"),
            P("sp", "tp"),
        ),
        check_vma=False,
    )
```

profile of v0, /device:TPU:1, one launch (start us, length us, event | category | flops | bytes accessed | tf_op | source)
XLA Modules:
  0.0 265.6 jit_solution(8091854053064930895)
XLA Ops:
  7.2 0.9 copy.133
  8.4 3.4 %mul.255 = f32[128,2,2048]{2,1,0:T(2,128)} broadcast(bf16[128,2048]{1,0:T(8,128)(2,1)} %param.17), dimensions={0,2} | broadcast | bytes 2621440 | tf_op jit(solution)/shard_map/mul | solution.py:241
  11.8 3.7 %mul.256 = f32[256,2048]{1,0:T(8,128)} reshape(f32[128,2,2048]{2,1,0:T(2,128)} %mul.255) | data formatting | bytes 4194304 | tf_op jit(solution)/shard_map/mul | solution.py:241
  15.7 0.6 reduce-window.6
  17.0 1.4 scatter_custom_fusion
  18.4 1.8 multiply_convert_fusion
  20.3 3.3 %gather_fusion.1 = bf16[512,2048]{1,0:T(8,128)(2,1)} fusion(bf16[257,2048]{1,0:T(8,128)(2,1)S(1)} %concatenate.13, s32[1024]{0:T(1024)S(1)} %get-tuple-element.222), kind=kCustom, calls=%fused_computation.1 | custom fusion | bytes 4196352 | tf_op jit(solution)/shard_map/gather | solution.py:249
  23.6 4.1 %copy.139 = bf16[32,16,2048]{2,0,1:T(8,128)(2,1)} copy(bf16[32,16,2048]{2,1,0:T(8,128)(2,1)} %bitcast.186) | data formatting | bytes 4194304 | tf_op jit(solution)/shard_map/reshape | solution.py:249
  27.8 3.3 %gather_fusion = bf16[512,2048]{1,0:T(8,128)(2,1)} fusion(bf16[129,2048]{1,0:T(8,128)(2,1)S(1)} %concatenate.12, s32[1024]{0:T(1024)S(1)} %get-tuple-element.223), kind=kCustom, calls=%fused_computation | custom fusion | bytes 4196352 | tf_op jit(solution)/shard_map/gather | solution.py:246
  31.1 2.9 %copy.138 = bf16[32,16,2048]{2,0,1:T(8,128)(2,1)S(1)} copy(bf16[32,16,2048]{2,1,0:T(8,128)(2,1)} %bitcast.187) | data formatting | bytes 4194304 | tf_op jit(solution)/shard_map/reshape | solution.py:246
  34.0 0.6 pad_maximum_fusion
  34.6 57.1 %all_to_all.20 = bf16[64,16,2048]{2,0,1:T(8,128)(2,1)S(1)} all-to-all(bf16[64,16,2048]{2,0,1:T(8,128)(2,1)S(1)} %pad_maximum_fusion), channel_id=1, replica_groups=mesh['sp'=16,'tp'=16] {'sp'}, dimensions={1} | all-to-all | bytes 8388608 | tf_op jit(solution)/shard_map/all_to_all | solution.py:13
  91.7 0.6 fusion.52
  92.3 1.2 copy.172
  93.5 1.3 fusion.7
  94.8 0.8 copy-done.8
  95.6 1.3 fusion.10
  96.9 1.2 copy.173
  98.1 0.5 copy-done.18
  98.6 1.5 multiply_convert_fusion.2
  100.1 1.3 fusion.5
  101.4 1.3 add_convert_fusion
  102.7 2.5 copy.142
  105.2 4.4 %all-to-all-start.1 = ((bf16[32,16,2048]{2,0,1:T(8,128)(2,1)}), bf16[32,16,2048]{2,0,1:T(8,128)(2,1)}, u32[]{:S(2)}, u32[]{:S(2)}) async-start(bf16[32,16,2048]{2,0,1:T(8,128)(2,1)} %copy.142), calls=%async_computation.1 | async-start | bytes 4194304 | tf_op jit(solution)/shard_map/all_to_all | solution.py:261
  109.7 27.2 %all-to-all-done.1 = bf16[32,16,2048]{2,0,1:T(8,128)(2,1)} async-done(((bf16[32,16,2048]{2,0,1:T(8,128)(2,1)}), bf16[32,16,2048]{2,0,1:T(8,128)(2,1)}, u32[]{:S(2)}, u32[]{:S(2)}) %all-to-all-start.1) | async-done | bytes 2097184 | tf_op jit(solution)/shard_map/all_to_all | solution.py:261
  136.9 4.7 %copy.143 = f32[32,16,2048]{2,1,0:T(8,128)} copy(bf16[32,16,2048]{2,0,1:T(8,128)(2,1)} %all-to-all-done.1) | data formatting | bytes 6291456 | tf_op jit(solution)/shard_map/reshape | solution.py:265
  141.6 5.8 %gather_fusion.2 = f32[256,2048]{1,0:T(8,128)} fusion(f32[512,2048]{1,0:T(8,128)} %bitcast.185, s32[1024]{0:T(1024)S(1)} %pad_clamp_fusion), kind=kCustom, calls=%fused_computation.2 | custom fusion | bytes 4195328 | tf_op jit(solution)/shard_map/gather | solution.py:267
  147.4 3.5 %reshape.393 = f32[128,2,2048]{2,1,0:T(2,128)} reshape(f32[256,2048]{1,0:T(8,128)} %gather_fusion.2) | data formatting | bytes 4194304 | tf_op jit(solution)/shard_map/reshape | solution.py:268
  150.9 5.0 %reduce_sum.55 = bf16[128,2048]{1,0:T(8,128)(2,1)} reduce(f32[128,2,2048]{2,1,0:T(2,128)} %reshape.393, f32[]{:T(128)} %constant.91.clone.1), dimensions={1}, to_apply=%region_4.5 | reduce | flops 262144 | bytes 2621444 | tf_op jit(solution)/shard_map/reduce_sum | solution.py:268
  156.8 4.2 %fusion.2 = bf16[1,2048,384]{2,1,0:T(8,128)(2,1)} fusion(bf16[512,2048]{1,0:T(8,128)(2,1)} %bitcast.199, bf16[512,384]{1,0:T(8,128)(2,1)S(1)} %get-tuple-element.210), kind=kOutput, calls=%fused_computation.15 | convolution fusion | flops 806092800 | bytes 4063232 | tf_op jit(solution)/shard_map/dot_general | solution.py:105
  161.0 2.5 fusion.3
  163.4 2.2 fusion.4
  165.7 49.1 %all-gather.3.cloned.1.call-done = bf16[2048,2048]{1,0:T(8,128)(2,1)} async-done(((bf16[128,2048]{1,0:T(8,128)(2,1)}), bf16[2048,2048]{1,0:T(8,128)(2,1)}) %all-gather.3.cloned.1.call-update) | async-done | bytes 8388624 | tf_op jit(solution)/shard_map/all_gather | solution.py:18
  214.7 5.3 %convert_reduce_fusion = f32[128,2048]{1,0:T(8,128)S(1)} fusion(bf16[16,128,2048]{2,1,0:T(8,128)(2,1)} %bitcast.188), kind=kLoop, calls=%fused_computation.9 | loop fusion | flops 8126464 | bytes 9437184 | tf_op jit(solution)/shard_map/reduce_sum | solution.py:19
  220.1 1.1 convolution_convert_fusion.3
  221.3 6.7 %all-to-all-start.2 = ((bf16[16,128,128]{2,1,0:T(8,128)(2,1)}), bf16[16,128,128]{2,1,0:T(8,128)(2,1)S(1)}, u32[]{:S(2)}, u32[]{:S(2)}) async-start(bf16[16,128,128]{2,1,0:T(8,128)(2,1)} %bitcast.15), calls=%async_computation.2 | async-start | bytes 1048576 | tf_op jit(solution)/shard_map/all_to_all | solution.py:30
  227.9 0.3 fusion.51
  229.1 9.7 %all-to-all-done.2 = bf16[16,128,128]{2,1,0:T(8,128)(2,1)S(1)} async-done(((bf16[16,128,128]{2,1,0:T(8,128)(2,1)}), bf16[16,128,128]{2,1,0:T(8,128)(2,1)S(1)}, u32[]{:S(2)}, u32[]{:S(2)}) %all-to-all-start.2) | async-done | bytes 524320 | tf_op jit(solution)/shard_map/all_to_all | solution.py:30
  238.7 0.8 broadcast_in_dim.88
  239.6 3.6 %all-to-all-start.3 = ((f32[16,65,128]{2,1,0:T(8,128)}), f32[16,65,128]{2,1,0:T(8,128)S(1)}, u32[]{:S(2)}, u32[]{:S(2)}) async-start(f32[16,65,128]{2,1,0:T(8,128)} %broadcast_in_dim.88), calls=%async_computation.3 | async-start | bytes 1179648 | tf_op jit(solution)/shard_map/all_to_all | solution.py:36
  243.3 0.3 convolution_multiply_fusion
  243.7 0.7 convert_reduce_fusion.1
  244.4 9.5 %all-to-all-done.3 = f32[16,65,128]{2,1,0:T(8,128)S(1)} async-done(((f32[16,65,128]{2,1,0:T(8,128)}), f32[16,65,128]{2,1,0:T(8,128)S(1)}, u32[]{:S(2)}, u32[]{:S(2)}) %all-to-all-start.3) | async-done | bytes 532512 | tf_op jit(solution)/shard_map/all_to_all | solution.py:36
  255.2 0.7 convert_element_type.129
  255.9 0.7 convert_element_type.132
  256.6 0.8 fusion.23
  257.7 0.3 fusion.24
  258.0 0.7 copy.164
  (124 shorter events, 5.0 us)
Async XLA Ops:
  7.2 86.3 %copy-start = (bf16[1,2048,384]{2,1,0:T(8,128)(2,1)S(1)}, bf16[1,2048,384]{2,1,0:T(8,128)(2,1)}, u32[]{:S(2)}) copy-start(bf16[1,2048,384]{2,1,0:T(8,128)(2,1)} %param.20) | copy-start | bytes 4718596
  11.8 3.7 %copy-start.17 = (f32[128,2]{0,1:T(2,128)S(1)}, f32[128,2]{0,1:T(2,128)}, u32[]{:S(2)}) copy-start(f32[128,2]{0,1:T(2,128)} %param.19) | copy-start | bytes 3076
  23.6 4.1 %copy-start.9 = (bf16[128,2048]{1,0:T(8,128)(2,1)S(1)}, bf16[128,2048]{1,0:T(8,128)(2,1)}, u32[]{:S(2)}) copy-start(bf16[128,2048]{1,0:T(8,128)(2,1)} %param.16) | copy-start | bytes 1572868
  31.1 2.9 %copy-start.2 = (bf16[32,16,2048]{2,0,1:T(8,128)(2,1)S(1)}, bf16[32,16,2048]{2,0,1:T(8,128)(2,1)}, u32[]{:S(2)}) copy-start(bf16[32,16,2048]{2,0,1:T(8,128)(2,1)} %copy.139) | copy-start | bytes 6291460
  93.4 1.4 copy-start.4
  93.5 2.2 copy-start.8
  95.6 2.5 copy-start.19
  96.9 1.2 copy-start.21
  96.9 1.7 copy-start.18
  98.1 2.0 copy-start.6
  105.2 31.7 %all-to-all-start.1 = ((bf16[32,16,2048]{2,0,1:T(8,128)(2,1)}), bf16[32,16,2048]{2,0,1:T(8,128)(2,1)}, u32[]{:S(2)}, u32[]{:S(2)}) async-start(bf16[32,16,2048]{2,0,1:T(8,128)(2,1)} %copy.142), calls=%async_computation.1 | async-start | bytes 4194304 | tf_op jit(solution)/shard_map/all_to_all | solution.py:261
  109.6 105.1 %all-gather.3.cloned.1.call-start = ((), (), s32[]{:S(2)}) async-start(), calls=%async_computation.4 | async-start | bytes 8912896 | tf_op jit(solution)/shard_map/all_gather | solution.py:18
  150.9 5.0 %copy-start.13 = (bf16[128,64]{0,1:T(8,128)(2,1)S(1)}, bf16[128,64]{0,1:T(8,128)(2,1)}, u32[]{:S(2)}) copy-start(bf16[128,64]{0,1:T(8,128)(2,1)} %param.26) | copy-start | bytes 49156
  150.9 5.3 %copy-start.14 = (bf16[128,64]{0,1:T(8,128)(2,1)S(1)}, bf16[128,64]{0,1:T(8,128)(2,1)}, u32[]{:S(2)}) copy-start(bf16[128,64]{0,1:T(8,128)(2,1)} %param.25) | copy-start | bytes 49156
  150.9 5.5 %copy-start.16 = (f32[128,64]{0,1:T(8,128)S(1)}, f32[128,64]{0,1:T(8,128)}, u32[]{:S(2)}) copy-start(f32[128,64]{0,1:T(8,128)} %param.28) | copy-start | bytes 98308
  156.8 4.2 %copy-start.5 = (bf16[32,16,2048]{2,1,0:T(8,128)(2,1)S(1)}, bf16[32,16,2048]{2,1,0:T(8,128)(2,1)}, u32[]{:S(2)}) copy-start(bf16[32,16,2048]{2,1,0:T(8,128)(2,1)} %copy-done.4) | copy-start | bytes 6291460
  161.0 2.5 copy-start.7
  161.0 2.5 copy-start.20
  161.0 2.5 copy-start.22
  214.7 5.4 %copy-start.3 = (bf16[128,2048]{1,0:T(8,128)(2,1)S(1)}, bf16[128,2048]{1,0:T(8,128)(2,1)}, u32[]{:S(2)}) copy-start(bf16[128,2048]{1,0:T(8,128)(2,1)} %param.17) | copy-start | bytes 1572868
  214.7 5.4 %copy-start.15 = (bf16[128,128]{1,0:T(8,128)(2,1)S(1)}, bf16[128,128]{1,0:T(8,128)(2,1)}, u32[]{:S(2)}) copy-start(bf16[128,128]{1,0:T(8,128)(2,1)} %param.24) | copy-start | bytes 98308
  220.1 7.8 %copy-start.10 = (bf16[128,2048]{1,0:T(8,128)(2,1)S(1)}, bf16[128,2048]{1,0:T(8,128)(2,1)}, u32[]{:S(2)}) copy-start(bf16[128,2048]{1,0:T(8,128)(2,1)} %param.23) | copy-start | bytes 1572868
  221.3 7.5 %copy-start.11 = (bf16[128,128]{1,0:T(8,128)(2,1)S(1)}, bf16[128,128]{1,0:T(8,128)(2,1)}, u32[]{:S(2)}) copy-start(bf16[128,128]{1,0:T(8,128)(2,1)} %param.27) | copy-start | bytes 98308
  221.3 17.5 %all-to-all-start.2 = ((bf16[16,128,128]{2,1,0:T(8,128)(2,1)}), bf16[16,128,128]{2,1,0:T(8,128)(2,1)S(1)}, u32[]{:S(2)}, u32[]{:S(2)}) async-start(bf16[16,128,128]{2,1,0:T(8,128)(2,1)} %bitcast.15), calls=%async_computation.2 | async-start | bytes 1048576 | tf_op jit(solution)/shard_map/all_to_all | solution.py:30
  228.3 14.9 %copy-start.12 = (f32[2,64,128]{2,1,0:T(8,128)S(1)}, f32[2,64,128]{2,1,0:T(8,128)}, u32[]{:S(2)}) copy-start(f32[2,64,128]{2,1,0:T(8,128)} %param.29) | copy-start | bytes 196612
  239.6 14.3 %all-to-all-start.3 = ((f32[16,65,128]{2,1,0:T(8,128)}), f32[16,65,128]{2,1,0:T(8,128)S(1)}, u32[]{:S(2)}, u32[]{:S(2)}) async-start(f32[16,65,128]{2,1,0:T(8,128)} %broadcast_in_dim.88), calls=%async_computation.3 | async-start | bytes 1179648 | tf_op jit(solution)/shard_map/all_to_all | solution.py:36
  254.2 4.5 %copy-start.1 = (bf16[1,2048,384]{2,1,0:T(8,128)(2,1)S(1)}, bf16[1,2048,384]{2,1,0:T(8,128)(2,1)}, u32[]{:S(2)}) copy-start(bf16[1,2048,384]{2,1,0:T(8,128)(2,1)} %param.20) | copy-start | bytes 4718596
Sparse Core Ops, SparseCore 0:
  156.0 58.6 all-gather.2
where the time goes:
time: 266 us
  waiting for transfers between devices  95.4 us (36%)
  blocking collectives  57.1 us (21%)
  local copies, waits for them, and re-layouts  49 us (18%)
  matrix products  19.5 us (7%)
  other arithmetic  15.2 us (6%)
  starting transfers between devices  14.7 us (6%)
  between operations  14.7 us (6%)
    all_to_all x1, blocking collectives, in_one_piece(): lax.all_to_all(both, axis, split_axis=split_dim, concat_axis=concat_dim,...  57.1 us
    all_gather x1, waiting for transfers between devices, over_pieces(): parts = lax.all_gather(shard, axis).astype(jnp.float32)  49.1 us
    all_to_all x1, waiting for transfers between devices, on_device(): lax.all_to_all(partial_value.astype(jnp.bfloat16), 'sp', split_axis=1, co...  27.2 us
    all_to_all x1, waiting for transfers between devices, sum_at_owner(): lax.all_to_all(parts, axis, split_axis=0, concat_axis=0, tiled=True)  9.65 us
    all_to_all x1, waiting for transfers between devices, copy_for_each(): lax.all_to_all(jnp.broadcast_to(shard[None], (length, *shard.shape)), axi...  9.47 us
    mul x3, local copies, waits for them, and re-layouts, on_device(): route_weight[:, :, None] * cotangent[:, None, :].astype(jnp.float32)  7.24 us
    all_to_all x1, starting transfers between devices, sum_at_owner(): lax.all_to_all(parts, axis, split_axis=0, concat_axis=0, tiled=True)  6.65 us
    gather x1, local copies, waits for them, and re-layouts, on_device(): picked = returned[rows_index]  5.78 us
  transfers between devices with their start and end apart: 4, of which 4 were waited for; matrix products, arithmetic and copies ran while one was open for 4% of the time, Pallas kernels for 0%

commit v1 on v0

--- a/solution.py
+++ b/solution.py
@@ -230,44 +230,53 @@
 ):
     tok_rows, width = moe_input.shape
     groups = lax.axis_size("sp")
+    lanes = lax.axis_size("tp")
     capacity = 4 * tok_rows // groups
+    part = width // lanes
+    offset = lax.axis_index("tp") * part
+    slots = groups * capacity
     target_locations = slot_places(route_expert, groups)
-    rows_index = (target_locations * groups + route_expert).reshape(-1)
-    owner = (
-        jnp.full((capacity * groups,), 2 * tok_rows, jnp.int32)
-        .at[rows_index]
-        .set(jnp.arange(2 * tok_rows, dtype=jnp.int32))
-    )
-    weighted = (route_weight[:, :, None] * cotangent[:, None, :].astype(jnp.float32)).astype(
-        jnp.bfloat16
-    )
-    weighted = weighted.reshape(2 * tok_rows, width)
-    blank = jnp.zeros((1, width), jnp.bfloat16)
-    send_in = jnp.concatenate([moe_input, blank], axis=0)[owner // 2].reshape(
-        capacity, groups, width
-    )
-    send_cot = jnp.concatenate([weighted, blank], axis=0)[owner].reshape(capacity, groups, width)
+    slot_index = route_expert * capacity + target_locations
+    numbers = jnp.arange(slots, dtype=jnp.int32)
+    chosen = [(numbers[:, None] == slot_index[None, :, j]).astype(jnp.bfloat16) for j in (0, 1)]
+    my_input = lax.dynamic_slice(moe_input, (0, offset), (tok_rows, part))
+    my_cot = lax.dynamic_slice(cotangent, (0, offset), (tok_rows, part))
+    weighted = [
+        (route_weight[:, j : j + 1] * my_cot.astype(jnp.float32)).astype(jnp.bfloat16)
+        for j in (0, 1)
+    ]
+    send_in = jnp.dot(chosen[0] + chosen[1], my_input, preferred_element_type=jnp.float32)
+    send_cot = jnp.dot(
+        jnp.concatenate(chosen, axis=1),
+        jnp.concatenate(weighted, axis=0),
+        preferred_element_type=jnp.float32,
+    )
+    send = jnp.concatenate([send_in, send_cot], axis=1).astype(jnp.bfloat16)
+    got = lax.all_to_all(
+        send.reshape(groups, capacity, 2 * part), "sp", split_axis=0, concat_axis=0, tiled=True
+    ).reshape(slots, 2 * part)
+    rows = lax.all_gather(got, "tp")
+    got_in = rows[:, :, :part].transpose(1, 0, 2).reshape(slots, width)
+    got_cot = rows[:, :, part:].transpose(1, 0, 2).reshape(slots, width)
     gate_weight = w_gate[0]
     up_weight = w_up[0]
     down_weight = w_down[0]
-    got_in, got_cot = in_one_piece((send_in, send_cot), "sp", 1, 1, 0)
     d_gate, d_upper, grad_gate, grad_up, grad_down = expert_grads(
-        got_in.reshape(-1, width), got_cot.reshape(-1, width), gate_weight, up_weight, down_weight
-    )
-    partial_value = input_grad(d_gate, d_upper, gate_weight, up_weight).reshape(
-        capacity, groups, width
-    )
-    returned = (
-        lax.all_to_all(
-            partial_value.astype(jnp.bfloat16), "sp", split_axis=1, concat_axis=1, tiled=True
-        )
-        .astype(partial_value.dtype)
-        .reshape(-1, width)
-    )
-    picked = returned[rows_index]
-    routed = jnp.sum(picked.reshape(tok_rows, 2, width), axis=1)
-    total = over_pieces(routed.astype(jnp.bfloat16), "tp").astype(jnp.float32)
-    grad_in = (cotangent.astype(jnp.float32) + total).astype(jnp.bfloat16)
+        got_in, got_cot, gate_weight, up_weight, down_weight
+    )
+    partial_value = input_grad(d_gate, d_upper, gate_weight, up_weight).astype(jnp.bfloat16)
+    mine = lax.psum_scatter(partial_value, "tp", scatter_dimension=1, tiled=True)
+    returned = lax.all_to_all(
+        mine.reshape(groups, capacity, part), "sp", split_axis=0, concat_axis=0, tiled=True
+    ).reshape(slots, part)
+    routed = lax.dot_general(
+        chosen[0] + chosen[1],
+        returned,
+        (((0,), (0,)), ((), ())),
+        preferred_element_type=jnp.float32,
+    )
+    grad_in = (my_cot.astype(jnp.float32) + routed).astype(jnp.bfloat16)
+    grad_in = lax.all_gather(grad_in, "tp", axis=1, tiled=True)
     grad_mix = lax.dot_general(
         grad_in, out_proj, (((1,), (1,)), ((), ())), preferred_element_type=jnp.float32
     )

time: 266 us -> 238 us (0.89)
  local copies, waits for them, and re-layouts: 49 us -> 26.4 us
  blocking collectives: 57.1 us -> 35.9 us
  waiting for transfers between devices: 95.4 us -> 111 us
  matrix products: 19.5 us -> 31.5 us
  other arithmetic: 15.2 us -> 4.14 us
    unnamed x1 -> x3, waiting for transfers between devices: 0.02 us -> 46.3 us
    all_to_all x1, blocking collectives: 57.1 us -> 15 us  [on_device(): lax.all_to_all(send.reshape(groups, capacity, 2 * part), 'sp', split_axis...]
    all_to_all x1, waiting for transfers between devices: 27.2 us -> 2.8 us  [on_device(): lax.all_to_all(mine.reshape(groups, capacity, part), 'sp', split_axis=0,...]
    all_gather x0 -> x1, blocking collectives: none -> 20.8 us  [on_device(): grad_in = lax.all_gather(grad_in, 'tp', axis=1, tiled=True)]
    reshape x5 -> x2, local copies, waits for them, and re-layouts: 15.4 us -> 0.2 us  [slot_places(): return jnp.sum(earlier * one_hot, axis=1).reshape(experts.shape)]
    gather x3 -> x0, local copies, waits for them, and re-layouts: 12.4 us -> none  [the longest x1 5.78 us: on_device(): picked = returned[rows_index]]
    reduce_sum x2 -> x0, other arithmetic: 10.3 us -> none  [the longest x1 5.34 us: over_pieces(): return parts.sum(axis=0)]
    unnamed x51 -> x46, local copies, waits for them, and re-layouts: 5.5 us -> 15.7 us
  transfers between devices with their start and end apart: 4 -> 5, of which waited for: 4 -> 5; matrix products, arithmetic and copies ran while one was open for 4% -> 7% of each run, Pallas kernels for 0% -> 0%
where the time goes in v1:
time: 238 us; the launch traced here: 237 us
  waiting for transfers between devices  111 us (47%)
  blocking collectives  35.9 us (15%)
  matrix products  31.5 us (13%)
  local copies, waits for them, and re-layouts  26.4 us (11%)
  between operations  14.5 us (6%)
  starting transfers between devices  13.6 us (6%)
  other arithmetic  4.14 us (2%)
    unnamed x3, waiting for transfers between devices  46.3 us
    all_gather x1, waiting for transfers between devices, on_device(): rows = lax.all_gather(got, 'tp')  42.8 us
    all_gather x1, blocking collectives, on_device(): grad_in = lax.all_gather(grad_in, 'tp', axis=1, tiled=True)  20.8 us
    unnamed x46, local copies, waits for them, and re-layouts  15.7 us
    all_to_all x1, blocking collectives, on_device(): lax.all_to_all(send.reshape(groups, capacity, 2 * part), 'sp', split_axis...  15 us
    all_to_all x1, waiting for transfers between devices, copy_for_each(): lax.all_to_all(jnp.broadcast_to(shard[None], (length, *shard.shape)), axi...  9.82 us
    all_to_all x1, waiting for transfers between devices, sum_at_owner(): lax.all_to_all(parts, axis, split_axis=0, concat_axis=0, tiled=True)  8.91 us
    all_to_all x1, starting transfers between devices, on_device(): lax.all_to_all(mine.reshape(groups, capacity, part), 'sp', split_axis=0,...  6.41 us
  transfers between devices with their start and end apart: 5, of which 5 were waited for; matrix products, arithmetic and copies ran while one was open for 7% of the time, Pallas kernels for 0%

profile of v1, /device:TPU:1, one launch (start us, length us, event | category | flops | bytes accessed | tf_op | source)
XLA Modules:
  0.0 236.7 jit_solution(16268379634097351561)
XLA Ops:
  7.2 0.9 copy.131
  8.4 0.6 reduce-window.6
  9.5 0.7 multiply_add_fusion.3
  10.3 0.8 slice_bitcast_fusion.3
  11.1 0.9 convolution_convert_fusion.5
  12.0 0.9 fusion.34
  12.9 0.2 convolution_convert_fusion.4
  13.2 15.0 %all_to_all.20 = bf16[16,32,256]{2,1,0:T(8,128)(2,1)} all-to-all(bf16[16,32,256]{2,1,0:T(8,128)(2,1)S(1)} %pad_maximum_fusion), channel_id=1, replica_groups=mesh['sp'=16,'tp'=16] {'sp'}, dimensions={0} | all-to-all | bytes 524288 | tf_op jit(solution)/shard_map/all_to_all | solution.py:255
  28.3 42.8 %all-gather.2.cloned.1.call-done = bf16[16,512,256]{2,1,0:T(8,128)(2,1)} async-done(((bf16[1,512,256]{2,1,0:T(8,128)(2,1)}), bf16[16,512,256]{2,1,0:T(8,128)(2,1)}) %all-gather.2.cloned.1.call-update) | async-done | bytes 4194320 | tf_op jit(solution)/shard_map/all_gather | solution.py:258
  71.1 4.7 %fusion.66 = (bf16[16,512,128]{2,1,0:T(8,128)(2,1)}, bf16[16,512,128]{2,1,0:T(8,128)(2,1)}) fusion(bf16[16,512,256]{2,1,0:T(8,128)(2,1)} %all-gather.2.cloned.1.call-done), kind=kLoop, calls=%fused_computation.123 | loop fusion | bytes 8388608 | tf_op jit(solution)/shard_map/slice | solution.py:260
  75.8 3.9 %copy.167 = bf16[16,512,128]{1,2,0:T(8,128)(2,1)} copy(bf16[16,512,128]{2,1,0:T(8,128)(2,1)} %get-tuple-element.208) | data formatting | bytes 4194304
  79.7 3.9 %fusion.7 = f32[512,384]{1,0:T(8,128)} fusion(bf16[512,2048]{0,1:T(8,128)(2,1)} %bitcast.200, bf16[1,2048,384]{2,1,0:T(8,128)(2,1)S(1)} %copy-done), kind=kOutput, calls=%fused_computation.15 | convolution fusion | flops 805306368 | bytes 4456448 | tf_op jit(solution)/shard_map/dot_general | solution.py:90
  83.6 2.2 fusion.10
  85.8 3.9 %copy.168 = bf16[16,512,128]{1,2,0:T(8,128)(2,1)} copy(bf16[16,512,128]{2,1,0:T(8,128)(2,1)} %get-tuple-element.207) | data formatting | bytes 4194304
  89.7 3.9 %multiply_convert_fusion.1 = (bf16[512,384]{1,0:T(8,128)(2,1)S(1)}, bf16[512,384]{1,0:T(8,128)(2,1)S(1)}) fusion(f32[512,384]{1,0:T(8,128)} %fusion.7, f32[512,384]{1,0:T(8,128)} %fusion.10, bf16[512,2048]{0,1:T(8,128)(2,1)} %bitcast.212, bf16[1,384,2048]{2,1,0:T(8,128)(2,1)} %param.22), kind=kOutput, calls=%fused_computation.48 | convolution fusion | flops 807862272 | bytes 6029312 | tf_op jit(solution)/shard_map/dot_general | solution.py:95
  93.6 1.3 fusion.5
  94.9 2.7 %add_convert_fusion = bf16[512,2048]{1,0:T(8,128)(2,1)} fusion(f32[512,2048]{1,0:T(8,128)S(1)} %fusion.5, bf16[512,384]{1,0:T(8,128)(2,1)S(1)} %get-tuple-element.209, bf16[1,2048,384]{2,1,0:T(8,128)(2,1)S(1)} %copy-done.2), kind=kOutput, calls=%fused_computation.5 | convolution fusion | flops 807403520 | bytes 8257536 | tf_op jit(solution)/shard_map/dot_general | solution.py:118
  97.6 3.9 %copy.165 = bf16[512,2048]{0,1:T(8,128)(2,1)} copy(bf16[512,2048]{1,0:T(8,128)(2,1)} %add_convert_fusion) | data formatting | bytes 4194304
  101.5 0.7 copy-done.12
  102.2 0.7 reshape.352
  103.0 0.7 reshape.351
  104.3 4.1 %fusion.2 = bf16[1,2048,384]{2,1,0:T(8,128)(2,1)} fusion(bf16[512,2048]{0,1:T(8,128)(2,1)} %bitcast.201, bf16[512,384]{1,0:T(8,128)(2,1)S(1)} %get-tuple-element.210), kind=kOutput, calls=%fused_computation.9 | convolution fusion | flops 806092800 | bytes 4063232 | tf_op jit(solution)/shard_map/dot_general | solution.py:105
  108.4 2.2 fusion.4
  110.7 46.2 %reduce-scatter.4.cloned.1.call-done = bf16[128,512]{1,0:T(8,128)(2,1)} async-done(((bf16[2048,512]{1,0:T(8,128)(2,1)}), bf16[128,512]{1,0:T(8,128)(2,1)}) %reduce-scatter.4.cloned.1.call-update) | async-done | bytes 131088
  156.9 1.7 copy.166
  158.5 6.4 %all-to-all-start.1 = ((bf16[16,32,128]{2,1,0:T(8,128)(2,1)}), bf16[16,32,128]{2,1,0:T(8,128)(2,1)S(1)}, u32[]{:S(2)}, u32[]{:S(2)}) async-start(bf16[16,32,128]{2,1,0:T(8,128)(2,1)} %bitcast.20), calls=%async_computation.1 | async-start | bytes 262144 | tf_op jit(solution)/shard_map/all_to_all | solution.py:269
  165.0 4.0 %fusion.3 = bf16[1,2048,384]{2,1,0:T(8,128)(2,1)} fusion(bf16[512,2048]{0,1:T(8,128)(2,1)} %bitcast.202, bf16[512,384]{1,0:T(8,128)(2,1)S(1)} %copy-done.7), kind=kOutput, calls=%fused_computation.10 | convolution fusion | flops 806092800 | bytes 4063232 | tf_op jit(solution)/shard_map/dot_general | solution.py:108
  169.0 2.8 %all-to-all-done.1 = bf16[16,32,128]{2,1,0:T(8,128)(2,1)S(1)} async-done(((bf16[16,32,128]{2,1,0:T(8,128)(2,1)}), bf16[16,32,128]{2,1,0:T(8,128)(2,1)S(1)}, u32[]{:S(2)}, u32[]{:S(2)}) %all-to-all-start.1) | async-done | bytes 131104 | tf_op jit(solution)/shard_map/all_to_all | solution.py:269
  171.8 1.0 fusion.23
  172.8 20.8 %all_gather.7 = bf16[128,2048]{1,0:T(8,128)(2,1)S(1)} all-gather(bf16[128,128]{1,0:T(8,128)(2,1)S(1)} %fusion.23), channel_id=1, replica_groups=mesh['sp'=16,'tp'=16] {'tp'}, dimensions={1}, use_global_device_ids=true | all-gather | bytes 557056 | tf_op jit(solution)/shard_map/all_gather | solution.py:279
  193.7 1.1 convolution_convert_fusion.3
  194.8 3.6 %all-to-all-start.2 = ((bf16[16,128,128]{2,1,0:T(8,128)(2,1)}), bf16[16,128,128]{2,1,0:T(8,128)(2,1)S(1)}, u32[]{:S(2)}, u32[]{:S(2)}) async-start(bf16[16,128,128]{2,1,0:T(8,128)(2,1)} %bitcast.22), calls=%async_computation.2 | async-start | bytes 1048576 | tf_op jit(solution)/shard_map/all_to_all | solution.py:30
  198.4 1.4 fusion.71
  200.0 0.2 while.17
  200.4 0.2 fusion.56
  200.6 8.9 %all-to-all-done.2 = bf16[16,128,128]{2,1,0:T(8,128)(2,1)S(1)} async-done(((bf16[16,128,128]{2,1,0:T(8,128)(2,1)}), bf16[16,128,128]{2,1,0:T(8,128)(2,1)S(1)}, u32[]{:S(2)}, u32[]{:S(2)}) %all-to-all-start.2) | async-done | bytes 524320 | tf_op jit(solution)/shard_map/all_to_all | solution.py:30
  209.5 0.9 broadcast_in_dim.73
  210.4 3.6 %all-to-all-start.3 = ((f32[16,65,128]{2,1,0:T(8,128)}), f32[16,65,128]{2,1,0:T(8,128)S(1)}, u32[]{:S(2)}, u32[]{:S(2)}) async-start(f32[16,65,128]{2,1,0:T(8,128)} %broadcast_in_dim.73), calls=%async_computation.3 | async-start | bytes 1179648 | tf_op jit(solution)/shard_map/all_to_all | solution.py:36
  214.1 0.3 convolution_multiply_fusion
  214.5 0.7 convert_reduce_fusion
  215.2 9.8 %all-to-all-done.3 = f32[16,65,128]{2,1,0:T(8,128)S(1)} async-done(((f32[16,65,128]{2,1,0:T(8,128)}), f32[16,65,128]{2,1,0:T(8,128)S(1)}, u32[]{:S(2)}, u32[]{:S(2)}) %all-to-all-start.3) | async-done | bytes 532512 | tf_op jit(solution)/shard_map/all_to_all | solution.py:36
  225.8 0.2 fusion.20
  226.1 0.2 fusion.41
  226.3 0.7 convert_element_type.118
  227.1 0.7 convert_element_type.121
  227.8 0.8 fusion.24
  228.8 0.3 fusion.25
  229.2 0.7 copy.157
  (107 shorter events, 3.5 us)
Async XLA Ops:
  7.2 72.5 %copy-start = (bf16[1,2048,384]{2,1,0:T(8,128)(2,1)S(1)}, bf16[1,2048,384]{2,1,0:T(8,128)(2,1)}, u32[]{:S(2)}) copy-start(bf16[1,2048,384]{2,1,0:T(8,128)(2,1)} %param.20) | copy-start | bytes 4718596
  7.2 63.9 %all-gather.2.cloned.1.call-start = ((), (), s32[]{:S(2)}) async-start(), calls=%async_computation.5 | async-start | bytes 4456448 | tf_op jit(solution)/shard_map/all_gather | solution.py:258
  10.3 65.5 %copy-start.16 = (s32[128]{0:T(128)}, s32[128]{0:T(128)S(1)}, u32[]{:S(2)}) copy-start(s32[128]{0:T(128)S(1)} %get-tuple-element.223) | copy-start | bytes 1540
  10.3 65.5 %copy-start.18 = (s32[128]{0:T(128)}, s32[128]{0:T(128)S(1)}, u32[]{:S(2)}) copy-start(s32[128]{0:T(128)S(1)} %get-tuple-element.224) | copy-start | bytes 1540
  28.2 128.7 %reduce-scatter.4.cloned.1.call-start = ((), (), s32[]{:S(2)}) async-start(), calls=%async_computation.6 | async-start | bytes 2228224
  79.7 3.9 %copy-start.1 = (bf16[16,512,128]{1,2,0:T(8,128)(2,1)S(1)}, bf16[16,512,128]{1,2,0:T(8,128)(2,1)}, u32[]{:S(2)}) copy-start(bf16[16,512,128]{1,2,0:T(8,128)(2,1)} %copy.167) | copy-start | bytes 6291460
  79.7 3.9 %copy-start.2 = (bf16[1,2048,384]{2,1,0:T(8,128)(2,1)S(1)}, bf16[1,2048,384]{2,1,0:T(8,128)(2,1)}, u32[]{:S(2)}) copy-start(bf16[1,2048,384]{2,1,0:T(8,128)(2,1)} %param.21) | copy-start | bytes 4718596
  93.6 1.3 copy-start.6
  101.5 0.7 copy-start.12
  101.5 1.6 copy-start.13
  101.5 2.4 %copy-start.14 = (f32[128,64]{0,1:T(8,128)S(1)}, f32[128,64]{0,1:T(8,128)}, u32[]{:S(2)}) copy-start(f32[128,64]{0,1:T(8,128)} %param.28) | copy-start | bytes 98308
  104.3 4.2 %copy-start.3 = (bf16[16,512,128]{1,2,0:T(8,128)(2,1)S(1)}, bf16[16,512,128]{1,2,0:T(8,128)(2,1)}, u32[]{:S(2)}) copy-start(bf16[16,512,128]{1,2,0:T(8,128)(2,1)} %copy.168) | copy-start | bytes 6291460
  104.3 4.2 %copy-start.4 = (f32[512,384]{1,0:T(8,128)S(1)}, f32[512,384]{1,0:T(8,128)}, u32[]{:S(2)}) copy-start(f32[512,384]{1,0:T(8,128)} %fusion.7) | copy-start | bytes 2359300
  104.3 4.2 %copy-start.5 = (f32[512,384]{1,0:T(8,128)S(1)}, f32[512,384]{1,0:T(8,128)}, u32[]{:S(2)}) copy-start(f32[512,384]{1,0:T(8,128)} %fusion.10) | copy-start | bytes 2359300
  108.4 56.5 %copy-start.7 = (bf16[512,384]{1,0:T(8,128)(2,1)S(1)}, bf16[512,384]{1,0:T(8,128)(2,1)}, u32[]{:S(2)}) copy-start(bf16[512,384]{1,0:T(8,128)(2,1)} %copy-done.6) | copy-start | bytes 1179652
  158.5 13.3 %all-to-all-start.1 = ((bf16[16,32,128]{2,1,0:T(8,128)(2,1)}), bf16[16,32,128]{2,1,0:T(8,128)(2,1)S(1)}, u32[]{:S(2)}, u32[]{:S(2)}) async-start(bf16[16,32,128]{2,1,0:T(8,128)(2,1)} %bitcast.20), calls=%async_computation.1 | async-start | bytes 262144 | tf_op jit(solution)/shard_map/all_to_all | solution.py:269
  165.0 6.8 %copy-start.17 = (s32[128]{0:T(128)S(1)}, s32[128]{0:T(128)}, u32[]{:S(2)}) copy-start(s32[128]{0:T(128)} %copy-done.16) | copy-start | bytes 1540
  165.0 6.8 %copy-start.19 = (s32[128]{0:T(128)S(1)}, s32[128]{0:T(128)}, u32[]{:S(2)}) copy-start(s32[128]{0:T(128)} %copy-done.18) | copy-start | bytes 1540
  165.0 28.7 %copy-start.15 = (bf16[128,128]{1,0:T(8,128)(2,1)S(1)}, bf16[128,128]{1,0:T(8,128)(2,1)}, u32[]{:S(2)}) copy-start(bf16[128,128]{1,0:T(8,128)(2,1)} %param.24) | copy-start | bytes 98308
  193.7 6.6 %copy-start.8 = (bf16[128,128]{1,0:T(8,128)(2,1)S(1)}, bf16[128,128]{1,0:T(8,128)(2,1)}, u32[]{:S(2)}) copy-start(bf16[128,128]{1,0:T(8,128)(2,1)} %param.27) | copy-start | bytes 98308
  194.8 14.7 %all-to-all-start.2 = ((bf16[16,128,128]{2,1,0:T(8,128)(2,1)}), bf16[16,128,128]{2,1,0:T(8,128)(2,1)S(1)}, u32[]{:S(2)}, u32[]{:S(2)}) async-start(bf16[16,128,128]{2,1,0:T(8,128)(2,1)} %bitcast.22), calls=%async_computation.2 | async-start | bytes 1048576 | tf_op jit(solution)/shard_map/all_to_all | solution.py:30
  198.4 15.6 %copy-start.11 = (f32[2,64,128]{2,1,0:T(8,128)S(1)}, f32[2,64,128]{2,1,0:T(8,128)}, u32[]{:S(2)}) copy-start(f32[2,64,128]{2,1,0:T(8,128)} %param.29) | copy-start | bytes 196612
  210.4 14.6 %all-to-all-start.3 = ((f32[16,65,128]{2,1,0:T(8,128)}), f32[16,65,128]{2,1,0:T(8,128)S(1)}, u32[]{:S(2)}, u32[]{:S(2)}) async-start(f32[16,65,128]{2,1,0:T(8,128)} %broadcast_in_dim.73), calls=%async_computation.3 | async-start | bytes 1179648 | tf_op jit(solution)/shard_map/all_to_all | solution.py:36
  215.2 10.9 %copy-start.9 = (f32[2,64,1,64]{1,0,3,2:T(2,128)S(1)}, f32[2,64,1,64]{1,0,3,2:T(2,128)}, u32[]{:S(2)}) copy-start(f32[2,64,1,64]{1,0,3,2:T(2,128)} %reshape.352) | copy-start | bytes 98308
  215.2 10.9 %copy-start.10 = (f32[2,64,1,64]{1,0,3,2:T(2,128)S(1)}, f32[2,64,1,64]{1,0,3,2:T(2,128)}, u32[]{:S(2)}) copy-start(f32[2,64,1,64]{1,0,3,2:T(2,128)} %reshape.351) | copy-start | bytes 98308
Sparse Core Ops, SparseCore 0:
  28.4 42.7 all-gather.1
  101.6 55.2 reduce-scatter.3

commit v2 on v0

v2 whole, which is shorter than its diff:
```python
import functools

import jax
import jax.numpy as jnp
from jax import lax
from jax.experimental import pallas as pl
from jax.experimental.pallas import tpu as pltpu
from jax.sharding import PartitionSpec as P

BF = jnp.bfloat16
F32 = jnp.float32
HIGH = lax.Precision.HIGHEST
LANE = 128
DK = 64
SPAN = 64
NN = (((1,), (0,)), ((), ()))
NT = (((1,), (1,)), ((), ()))
TN = (((0,), (0,)), ((), ()))


def mm(a, b, dims=NN, precision=None):
    return lax.dot_general(a, b, dims, precision=precision, preferred_element_type=F32)


def half_dot(a, b, dims=NN):
    return mm(a.astype(BF), b.astype(BF), dims)


def waited(ref, sem):
    pltpu.make_async_copy(ref, ref, sem).wait()


def main_kernel(
    route_ref, weight_ref, input_ref, cot_ref, proj_ref, saved_ref, q_ref, k_ref, v_ref, log_ref,
    state_ref, wg_hbm, wu_hbm, wd_hbm,
    rows_hbm, hid_hbm, dg_hbm, du_hbm, gproj_ref, gq_ref, gk_ref, gv_ref, gd_ref,
    wg, wu, wd, table, send, rows, gate_acc, up_acc, hid_acc, hid, dgu, tmp, mine, pair_out,
    pair_in, back_out, back_in, far_out, far_in, grad_in, pj_out, pj_in, pj_own, tot_out, tot_in,
    carry_out, carry_in, after,
    w_sem, out_sem, disp_s, disp_r, ring_s, ring_r, core_s, core_r, pair_s, pair_r, back_s, back_r,
    far_s, far_r, all_s, all_r, fwd_s, fwd_r, pj_s, pj_r, tot_s, tot_r, carry_s, carry_r,
    *, groups, lanes, capacity,
):
    chips = lanes // 2
    sp, tp = lax.axis_index("sp"), lax.axis_index("tp")
    z, core = lax.div(tp, 2), lax.rem(tp, 2)
    other = 1 - core
    tokens = input_ref.shape[0]
    slots = groups * capacity
    hidden = wg.shape[1]
    half = groups // 2

    def wrapped(rel):
        return lax.rem(z + rel, chips)

    def to(src, dst, send_sem, recv_sem, **where):
        pltpu.make_async_remote_copy(
            src_ref=src, dst_ref=dst, send_sem=send_sem, recv_sem=recv_sem,
            device_id=where, device_id_type=pl.DeviceIdType.MESH,
        ).start()

    def to_tp(src, dst, send_sem, recv_sem, chip, at_core):
        to(src, dst, send_sem, recv_sem, tp=chip * 2 + at_core)

    barrier = pltpu.get_barrier_semaphore()

    @pl.loop(1, groups)
    def _(o):
        pl.semaphore_signal(
            barrier, inc=1, device_id={"sp": lax.rem(sp + o, groups)},
            device_id_type=pl.DeviceIdType.MESH,
        )

    @pl.loop(1, chips)
    def _(o):
        pl.semaphore_signal(
            barrier, inc=1, device_id={"tp": wrapped(o) * 2 + core},
            device_id_type=pl.DeviceIdType.MESH,
        )

    pl.semaphore_signal(
        barrier, inc=1, device_id={"tp": z * 2 + other}, device_id_type=pl.DeviceIdType.MESH
    )

    copies = [
        pltpu.make_async_copy(wg_hbm.at[0], wg, w_sem.at[0]),
        pltpu.make_async_copy(wu_hbm.at[0], wu, w_sem.at[1]),
        pltpu.make_async_copy(wd_hbm.at[0], wd, w_sem.at[2]),
    ]
    for copy in copies:
        copy.start()

    experts = lax.broadcasted_iota(jnp.int32, (tokens, groups), 1)
    named = [(route_ref[:, j : j + 1] == experts).astype(F32) for j in (0, 1)]
    row = lax.broadcasted_iota(jnp.int32, (tokens, tokens), 0)
    col = lax.broadcasted_iota(jnp.int32, (tokens, tokens), 1)
    earlier = half_dot((row > col).astype(F32), named[0] + named[1])
    place_in = lax.broadcasted_iota(jnp.int32, (tokens, slots), 1)
    for j in (0, 1):
        place = jnp.sum(earlier * named[j], axis=1, keepdims=True).astype(jnp.int32)
        slot = route_ref[:, j : j + 1] * capacity + place
        table[j] = (slot == place_in).astype(F32).astype(BF)
    far_blocks = list(range(3, chips - 2)) if chips > 4 else [2]
    near = 2 if chips > 4 else 1
    firsts = [0] + far_blocks

    def fill(b, rel):
        t = wrapped(rel) * 2 + core
        columns = pl.ds(pl.multiple_of(t * LANE, LANE), LANE)
        cot = cot_ref[:, columns].astype(F32)
        first = table[0]
        second = table[1]
        ins = mm(first + second, input_ref[:, columns], TN)
        cots = mm(first, (weight_ref[:, 0:1] * cot).astype(BF), TN)
        cots += mm(second, (weight_ref[:, 1:2] * cot).astype(BF), TN)
        send[b, :, :capacity] = ins.astype(BF).reshape(groups, capacity, LANE)
        send[b, :, capacity:] = cots.astype(BF).reshape(groups, capacity, LANE)
        rows[t, sp] = send[b, sp]

    def dispatch(b, rel):
        t = wrapped(rel) * 2 + core

        @pl.loop(1, groups)
        def _(o):
            peer = lax.rem(sp + o, groups)
            to(send.at[b, peer], rows.at[t, sp], disp_s.at[b], disp_r.at[b], sp=peer)

    fill(0, 0)
    totals = jnp.sum(log_ref[...], axis=0, keepdims=True)
    tot_out[...] = jnp.concatenate(
        [jnp.broadcast_to(totals, (8, DK)), jnp.zeros((8, LANE - DK), F32)], axis=1
    )
    tot_in[sp] = tot_out[...]
    pl.semaphore_wait(barrier, groups - 1 + chips)

    dispatch(0, 0)
    for b, rel in enumerate(firsts):
        if b:
            fill(b, rel)
            dispatch(b, rel)

    @pl.loop(1, groups)
    def _(o):
        peer = lax.rem(sp + o, groups)
        to(tot_out, tot_in.at[sp], tot_s, tot_r, sp=peer)

    gate_acc[...] = jnp.zeros_like(gate_acc)
    up_acc[...] = jnp.zeros_like(up_acc)
    hid_acc[...] = jnp.zeros_like(hid_acc)

    def halves(t, h):
        return rows.at[t, pl.ds(h * half, half)]

    def block(rel):
        return wrapped(rel) * 2 + core

    def pass_ring(rel, step, h, side):
        chip = wrapped(1 if side == 0 else chips - 1)
        part = halves(block(rel), h)
        to_tp(part, part, ring_s.at[step, side, h], ring_r.at[step, side, h], chip, core)

    def await_ring(rel, step, h, side):
        waited(halves(block(rel), h), ring_r.at[step, side, h])

    def to_other(rel):
        t = block(rel)
        to_tp(rows.at[t], rows.at[t], core_s.at[rel], core_r.at[rel], z, other)

    def from_other(rel):
        waited(rows.at[wrapped(rel) * 2 + other], core_r.at[rel])

    def both(zz, start):
        pieces = [
            rows[zz * 2 + k, :, start : start + capacity].reshape(slots, LANE) for k in (0, 1)
        ]
        return jnp.concatenate(pieces, axis=1)

    def gather_product(rel):
        zz = wrapped(rel)
        depth = pl.ds(pl.multiple_of(zz * 2 * LANE, 2 * LANE), 2 * LANE)
        ins = both(zz, 0)
        gate_acc[...] += mm(ins, wg[depth, :])
        up_acc[...] += mm(ins, wu[depth, :])
        hid_acc[...] += mm(both(zz, capacity), wd[:, depth], NT)

    def await_dispatch(b):
        waited(send.at[b, pl.ds(0, groups - 1)], disp_r.at[b])

    await_dispatch(0)
    for h in (0, 1):
        for side in (0, 1):
            pass_ring(0, 0, h, side)
    to_other(0)
    for copy in copies:
        copy.wait()
    from_other(0)
    gather_product(0)
    for h in (0, 1):
        for side in (0, 1):
            rel = chips - 1 if side == 0 else 1
            await_ring(rel, 0, h, side)
            if near > 1:
                pass_ring(rel, 1, h, side)
        if h == 0 and len(firsts) > 1:
            await_dispatch(1)
            to_other(firsts[1])
    to_other(1)
    to_other(chips - 1)
    for b, rel in enumerate(firsts):
        if b > 1:
            await_dispatch(b)
            to_other(rel)

    @pl.loop(0, len(far_blocks))
    def _(i):
        rel = far_blocks[0] + i
        from_other(rel)
        gather_product(rel)

    @pl.loop(0, 2)
    def _(i):
        rel = 1 + i * (chips - 2)
        from_other(rel)
        gather_product(rel)

    if near > 1:
        for side in (0, 1):
            rel = chips - 2 if side == 0 else 2
            for h in (0, 1):
                await_ring(rel, 1, h, side)
            to_other(rel)

        @pl.loop(0, 2)
        def _(i):
            rel = chips - 2 - i * (chips - 4)
            from_other(rel)
            gather_product(rel)

    rows_copy = pltpu.make_async_copy(rows, rows_hbm, out_sem.at[0])
    rows_copy.start()
    tile = 64

    @pl.loop(0, slots // tile)
    def _(i):
        at = pl.ds(pl.multiple_of(i * tile, tile), tile)
        gate = gate_acc[at, :]
        upper = up_acc[at, :]
        d_hidden = hid_acc[at, :]
        sigmoid = jax.nn.sigmoid(gate)
        active = gate * sigmoid
        hid[at, :] = (active * upper).astype(BF)
        dgu[at, hidden:] = (d_hidden * active).astype(BF)
        dgu[at, :hidden] = (
            d_hidden * upper * sigmoid * (1.0 + gate * (1.0 - sigmoid))
        ).astype(BF)

    out_copies = [
        pltpu.make_async_copy(hid, hid_hbm, out_sem.at[1]),
        pltpu.make_async_copy(dgu.at[:, pl.ds(0, hidden)], dg_hbm, out_sem.at[2]),
        pltpu.make_async_copy(dgu.at[:, pl.ds(hidden, hidden)], du_hbm, out_sem.at[3]),
    ]
    for copy in out_copies:
        copy.start()

    def far_first(j):
        return lax.rem(chips // 2 + lax.div(j + 1, 2) * (2 * lax.rem(j, 2) - 1), chips)

    def slot_block(j):
        zz = wrapped(far_first(j))
        depth = pl.ds(pl.multiple_of(zz * 2 * LANE, 2 * LANE), 2 * LANE)
        tmp[...] = mm(dgu[:, :hidden], wg[depth, :], NT) + mm(dgu[:, hidden:], wu[depth, :], NT)
        pair_out[j] = tmp[:, pl.ds(pl.multiple_of(other * LANE, LANE), LANE)].astype(BF)
        mine[j] = tmp[:, pl.ds(pl.multiple_of(core * LANE, LANE), LANE)]
        to_tp(pair_out.at[j], pair_in.at[j], pair_s.at[j], pair_r.at[j], z, other)

    def slot_return(j):
        waited(pair_in.at[j], pair_r.at[j])
        whole = (mine[j] + pair_in[j].astype(F32)).astype(BF)
        back_out[j] = whole.reshape(groups, capacity, LANE)
        back_in[j, sp] = back_out[j, sp]

        @pl.loop(1, groups)
        def _(o):
            peer = lax.rem(sp + o, groups)
            to(back_out.at[j, peer], back_in.at[j, sp], back_s.at[j], back_r.at[j], sp=peer)

    lag = 2

    @pl.loop(0, chips + lag)
    def _(j):
        @pl.when(j < chips)
        def _():
            slot_block(j)

        @pl.when(j >= lag)
        def _():
            slot_return(j - lag)

    def routed(j):
        waited(back_out.at[j, pl.ds(0, groups - 1)], back_r.at[j])
        return mm(table[0] + table[1], back_in[j].reshape(slots, LANE))

    @pl.loop(0, chips - 1)
    def _(j):
        rel = far_first(j)
        far_out[j] = routed(j).astype(BF)
        to_tp(far_out.at[j], far_in.at[rel], far_s.at[j], far_r.at[rel], wrapped(rel), core)

    total = routed(chips - 1)
    causal = ((row >= col) & (lax.div(row, SPAN) == lax.div(col, SPAN))).astype(F32)
    cum = mm(causal, log_ref[...], NN, HIGH)
    cum_t = mm(log_ref[...], causal, (((0,), (1,)), ((), ())), HIGH)
    waited(tot_in.at[pl.ds(0, groups - 1)], tot_r)
    after_row = lax.broadcasted_iota(jnp.int32, (groups, LANE), 0)
    after_col = lax.broadcasted_iota(jnp.int32, (groups, LANE), 1)
    between = ((after_row > after_col) & (after_row < sp)).astype(F32)
    factors = jnp.exp(mm(tot_in[:, 0, :DK], between, TN, HIGH))

    for rel in range(1, chips):
        waited(far_in.at[rel], far_r.at[rel])
        total += far_in[rel].astype(F32)
    columns = pl.ds(pl.multiple_of(tp * LANE, LANE), LANE)
    grad_in[tp] = (cot_ref[:, columns].astype(F32) + total).astype(BF)
    order = sorted(range(1, chips), key=lambda r: -min(r, chips - r))
    for rel in order:
        to_tp(grad_in.at[tp], grad_in.at[tp], all_s.at[rel], all_r.at[rel], wrapped(rel), core)
    to_tp(grad_in.at[tp], grad_in.at[tp], fwd_s.at[0], fwd_r.at[0], z, other)
    for rel in order[::-1]:
        t = wrapped(chips - rel) * 2 + core
        waited(grad_in.at[t], all_r.at[rel])
        to_tp(grad_in.at[t], grad_in.at[t], fwd_s.at[rel], fwd_r.at[rel], z, other)
    for rel in range(chips):
        waited(grad_in.at[wrapped(chips - rel if rel else 0) * 2 + other], fwd_r.at[rel])

    mix = jnp.zeros((tokens, LANE), F32)
    for zz in range(chips):
        pair = jnp.concatenate([grad_in[2 * zz], grad_in[2 * zz + 1]], axis=1)
        mix += mm(pair, proj_ref[:, 2 * zz * LANE : 2 * (zz + 1) * LANE], NT)

    scale = DK ** (-0.5)
    grown = jnp.exp(cum)
    shrunk = jnp.exp(-cum)
    queries = q_ref[...].astype(F32)
    keys = k_ref[...].astype(F32)
    qd = (queries * grown).astype(BF)
    kd = (keys * shrunk).astype(BF)
    mix_half = mix.astype(BF)
    spans = [slice(n * SPAN, (n + 1) * SPAN) for n in (0, 1)]
    local = [scale * mm(qd[s], mix_half[s], TN) for s in spans]
    last_t = [jnp.exp(cum_t[:, n * SPAN + SPAN - 1 : (n + 1) * SPAN]) for n in (0, 1)]
    begin = local[0] + last_t[0] * local[1]
    for r in range(groups - 1):
        @pl.when(sp > r)
        def _():
            carry_out[r] = (begin * factors[:, r : r + 1]).astype(BF)
            to(carry_out.at[r], carry_in.at[sp], carry_s.at[r], carry_r.at[sp], sp=r)

    @pl.loop(1, groups)
    def _(o):
        peer = lax.rem(sp + o, groups)
        pj_out[peer] = mm(grad_in[peer], saved_ref[...], TN).astype(BF)
        to(pj_out.at[peer], pj_in.at[sp], pj_s, pj_r, sp=peer)

    pj_own[...] = mm(grad_in[sp], saved_ref[...], TN)

    values = v_ref[...]
    ends = [cum[n * SPAN + SPAN - 1 : (n + 1) * SPAN] for n in (0, 1)]
    to_end = [jnp.exp(ends[n] - cum[spans[n]]) for n in (0, 1)]
    ke = [(keys[spans[n]] * to_end[n]).astype(BF) for n in (0, 1)]
    lower = causal[:SPAN, :SPAN]
    parts = []
    for n in (0, 1):
        s = spans[n]
        state = state_ref[n]
        scores = mm(qd[s], kd[s], NT) * lower
        dots = (mm(mix_half[s], values[s], NT) * lower).astype(BF)
        dq = scale * grown[s] * (mm(dots, kd[s]) + mm(mix_half[s], state.astype(BF), NT))
        dk = scale * shrunk[s] * mm(dots, qd[s], TN)
        dv = scale * mm(scores.astype(BF), mix_half[s], TN)
        state_end = last_t[n] * state + mm(ke[n], values[s], TN)
        parts.append((dq, dk, dv, state_end))

    after[...] = jnp.zeros_like(after)
    for s in range(1, groups):
        @pl.when(s > sp)
        def _():
            waited(carry_in.at[s], carry_r.at[s])
            after[...] += carry_in[s].astype(F32)

    end_1 = after[...]
    g_end = [local[1] + last_t[1] * end_1, end_1]
    upper_ones = (col[:SPAN, :SPAN] >= row[:SPAN, :SPAN]).astype(F32)
    for n in (0, 1):
        s = spans[n]
        dq, dk, dv, state_end = parts[n]
        end = g_end[n].astype(BF)
        dk = dk + to_end[n] * mm(values[s], end, NT)
        dv = dv + mm(ke[n], end)
        tail = mm(jnp.ones((8, LANE), F32), state_end * g_end[n], NT, HIGH)[:1]
        d_cum = queries[s] * dq - keys[s] * dk
        gd_ref[s, :] = mm(upper_ones, d_cum, NN, HIGH) + tail
        gq_ref[s, :] = dq.astype(BF)
        gk_ref[s, :] = dk.astype(BF)
        gv_ref[s, :] = dv.astype(BF)

    waited(pj_in.at[pl.ds(0, groups - 1)], pj_r)
    gproj_ref[...] = pj_own[...]

    @pl.loop(1, groups)
    def _(o):
        peer = lax.rem(sp + o, groups)
        gproj_ref[...] += pj_in[peer].astype(F32)

    for b in range(len(firsts)):
        waited(send.at[b, pl.ds(0, groups - 1)], disp_s.at[b])
    waited(tot_in.at[pl.ds(0, groups - 1)], tot_s)
    for step in range(near):
        for side in (0, 1):
            for h in (0, 1):
                waited(halves(0, h), ring_s.at[step, side, h])
    for rel in range(chips):
        waited(rows.at[0], core_s.at[rel])
        waited(pair_out.at[rel], pair_s.at[rel])
        waited(back_out.at[rel, pl.ds(0, groups - 1)], back_s.at[rel])
        waited(grad_in.at[0], fwd_s.at[rel])
        if rel:
            waited(far_out.at[0], far_s.at[rel - 1])
            waited(grad_in.at[0], all_s.at[rel])
    waited(pj_out.at[pl.ds(0, groups - 1)], pj_s)
    for r in range(groups - 1):
        @pl.when(sp > r)
        def _():
            waited(carry_out.at[r], carry_s.at[r])
    rows_copy.wait()
    for copy in out_copies:
        copy.wait()


def weight_kernel(rows, hid, dg, du, gp, gq, gk, gv, gd, gg, gu, gw, op, oq, ok, ov, od):
    slots = hid.shape[0]
    capacity = rows.shape[2] // 2

    def both(start):
        pieces = [rows[k, :, start : start + capacity].reshape(slots, LANE) for k in (0, 1)]
        return jnp.concatenate(pieces, axis=1)

    ins = both(0)
    gg[0] = mm(ins, dg[...], TN).astype(BF)
    gu[0] = mm(ins, du[...], TN).astype(BF)
    gw[0] = mm(hid[...], both(capacity), TN).astype(BF)

    @pl.when(pl.program_id(0) == 0)
    def _():
        for out, given in ((op, gp), (oq, gq), (ok, gk), (ov, gv), (od, gd)):
            out[...] = given[...]


def on_device(
    moe_input, cotangent, route_expert, route_weight, w_gate, w_up, w_down, out_proj, saved_out,
    queries, keys, values, log_decay, span_state,
):
    groups, lanes = lax.axis_size("sp"), lax.axis_size("tp")
    tokens, width = moe_input.shape
    capacity = 4 * tokens // groups
    slots = groups * capacity
    hidden = w_gate.shape[2]
    chips = lanes // 2
    firsts = 4 if chips > 4 else 2
    vmem = pl.BlockSpec(memory_space=pltpu.VMEM)
    hbm = pl.BlockSpec(memory_space=pl.ANY)
    dma = pltpu.SemaphoreType.DMA
    shape = jax.ShapeDtypeStruct
    slab = (groups, 2 * capacity, LANE)
    scratch = [
        pltpu.VMEM((width, hidden), BF),
        pltpu.VMEM((width, hidden), BF),
        pltpu.VMEM((hidden, width), BF),
        pltpu.VMEM((2, tokens, slots), BF),
        pltpu.VMEM((firsts, *slab), BF),
        pltpu.VMEM((lanes, *slab), BF),
        pltpu.VMEM((slots, hidden), F32),
        pltpu.VMEM((slots, hidden), F32),
        pltpu.VMEM((slots, hidden), F32),
        pltpu.VMEM((slots, hidden), BF),
        pltpu.VMEM((slots, 2 * hidden), BF),
        pltpu.VMEM((slots, 2 * LANE), F32),
        pltpu.VMEM((chips, slots, LANE), F32),
        pltpu.VMEM((chips, slots, LANE), BF),
        pltpu.VMEM((chips, slots, LANE), BF),
        pltpu.VMEM((chips, groups, capacity, LANE), BF),
        pltpu.VMEM((chips, groups, capacity, LANE), BF),
        pltpu.VMEM((chips, tokens, LANE), BF),
        pltpu.VMEM((chips, tokens, LANE), BF),
        pltpu.VMEM((lanes, tokens, LANE), BF),
        pltpu.VMEM((groups, LANE, LANE), BF),
        pltpu.VMEM((groups, LANE, LANE), BF),
        pltpu.VMEM((LANE, LANE), F32),
        pltpu.VMEM((8, LANE), F32),
        pltpu.VMEM((groups, 8, LANE), F32),
        pltpu.VMEM((groups, DK, LANE), BF),
        pltpu.VMEM((groups, DK, LANE), BF),
        pltpu.VMEM((DK, LANE), F32),
        dma((3,)), dma((4,)),
        dma((firsts,)), dma((firsts,)),
        dma((2, 2, 2)), dma((2, 2, 2)),
        dma((chips,)), dma((chips,)),
        dma((chips,)), dma((chips,)),
        dma((chips,)), dma((chips,)),
        dma((chips,)), dma((chips,)),
        dma((chips,)), dma((chips,)),
        dma((chips,)), dma((chips,)),
        dma, dma, dma, dma,
        dma((groups,)), dma((groups,)),
    ]
    rows, hid, dg, du, gp, gq, gk, gv, gd = pl.pallas_call(
        functools.partial(main_kernel, groups=groups, lanes=lanes, capacity=capacity),
        name="experts_and_attention",
        out_shape=(
            shape((lanes, *slab), BF),
            shape((slots, hidden), BF),
            shape((slots, hidden), BF),
            shape((slots, hidden), BF),
            shape((LANE, LANE), F32),
            shape((tokens, DK), BF),
            shape((tokens, DK), BF),
            shape((tokens, LANE), BF),
            shape((tokens, DK), F32),
        ),
        in_specs=[vmem] * 11 + [hbm] * 3,
        out_specs=(hbm,) * 4 + (vmem,) * 5,
        scratch_shapes=scratch,
        compiler_params=pltpu.CompilerParams(
            collective_id=0, has_side_effects=True, vmem_limit_bytes=56 * 1024 * 1024
        ),
    )(
        route_expert, route_weight, moe_input, cotangent, out_proj, saved_out, queries, keys,
        values, log_decay, span_state, w_gate, w_up, w_down,
    )
    small = (gp, gq, gk, gv, gd)

    def same(array):
        return pl.BlockSpec(array.shape, lambda i: (0,) * array.ndim)

    results = pl.pallas_call(
        weight_kernel,
        name="weight_grads",
        grid=(chips,),
        out_shape=(
            shape((1, width, hidden), BF),
            shape((1, width, hidden), BF),
            shape((1, hidden, width), BF),
            *(shape(a.shape, a.dtype) for a in small),
        ),
        in_specs=[
            pl.BlockSpec((2, *slab), lambda i: (i, 0, 0, 0)),
            *(same(a) for a in (hid, dg, du, *small)),
        ],
        out_specs=(
            pl.BlockSpec((1, 2 * LANE, hidden), lambda i: (0, i, 0)),
            pl.BlockSpec((1, 2 * LANE, hidden), lambda i: (0, i, 0)),
            pl.BlockSpec((1, hidden, 2 * LANE), lambda i: (0, 0, i)),
            *(same(a) for a in small),
        ),
        compiler_params=pltpu.CompilerParams(vmem_limit_bytes=32 * 1024 * 1024),
    )(rows, hid, dg, du, *small)
    return results


def solution(mesh):
    placed = (
        P("sp", None),
        P("sp", None),
        P("sp", None),
        P("sp", None),
        P("sp", None, "tp"),
        P("sp", None, "tp"),
        P("sp", "tp", None),
        P("tp", None),
        P("sp", "tp"),
        P("sp", "tp"),
        P("sp", "tp"),
        P("sp", "tp"),
        P("sp", "tp"),
        P("sp", "tp", None),
    )
    return jax.shard_map(
        on_device,
        mesh=mesh,
        in_specs=placed,
        out_specs=(
            P("sp", None, "tp"),
            P("sp", None, "tp"),
            P("sp", "tp", None),
            P("sp", "tp"),
            P("sp", "tp"),
            P("sp", "tp"),
            P("sp", "tp"),
            P("sp", "tp"),
        ),
        check_vma=False,
    )
```

time: 266 us -> 100 us (0.38)
  waiting for transfers between devices: 95.4 us -> 0 us
  Pallas kernels: 0 us -> 80.2 us
  blocking collectives: 57.1 us -> 0 us
  local copies, waits for them, and re-layouts: 49 us -> 18.4 us
  matrix products: 19.5 us -> 0 us
  other arithmetic: 15.2 us -> 0 us
  starting transfers between devices: 14.7 us -> 0 us
  between operations: 14.7 us -> 0.66 us
    pallas_call x0 -> x2, Pallas kernels: none -> 80.2 us  [the longest x1 74.1 us: on_device(): pl.pallas_call(functools.partial(main_kernel, groups=groups, lanes=lanes,...]
    all_to_all x1 -> x0, blocking collectives: 57.1 us -> none  [in_one_piece(): lax.all_to_all(both, axis, split_axis=split_dim, concat_axis=concat_dim,...]
    all_gather x1 -> x0, waiting for transfers between devices: 49.1 us -> none  [over_pieces(): parts = lax.all_gather(shard, axis).astype(jnp.float32)]
    all_to_all x3 -> x0, waiting for transfers between devices: 46.3 us -> none  [the longest x1 27.2 us: on_device(): lax.all_to_all(partial_value.astype(jnp.bfloat16), 'sp', split_axis=1, co...]
    dot_general x19 -> x0, matrix products: 19.5 us -> none  [the longest x1 4.18 us: expert_grads(): lax.dot_general(inputs, d_gate, (((0,), (0,)), ((), ())), preferred_eleme...]
    reshape x9 -> x0, local copies, waits for them, and re-layouts: 15.7 us -> none  [the longest x1 4.74 us: on_device(): returned = lax.all_to_all(partial_value.astype(jnp.bfloat16), 'sp', split...]
    all_to_all x3 -> x0, starting transfers between devices: 14.7 us -> none  [the longest x1 6.65 us: sum_at_owner(): lax.all_to_all(parts, axis, split_axis=0, concat_axis=0, tiled=True)]
    gather x3 -> x0, local copies, waits for them, and re-layouts: 12.4 us -> none  [the longest x1 5.78 us: on_device(): picked = returned[rows_index]]
  transfers between devices with their start and end apart: 4 -> 0, of which waited for: 4 -> 0; matrix products, arithmetic and copies ran while one was open for 4% -> 0% of each run, Pallas kernels for 0% -> 0%
where the time goes in v2:
time: 100 us; the launch traced here: 99.3 us
  Pallas kernels  80.2 us (80%)
  local copies, waits for them, and re-layouts  18.4 us (18%)
    pallas_call x1, Pallas kernels, on_device(): pl.pallas_call(functools.partial(main_kernel, groups=groups, lanes=lanes,...  74.1 us
    unnamed x23, local copies, waits for them, and re-layouts  16.3 us
    pallas_call x1, Pallas kernels, on_device(): pl.pallas_call(weight_kernel, name='weight_grads', grid=(chips,), out_sha...  6.13 us
    pallas_call x3, local copies, waits for them, and re-layouts, on_device(): pl.pallas_call(weight_kernel, name='weight_grads', grid=(chips,), out_sha...  2.09 us

profile of v2, /device:TPU:1, one launch (start us, length us, event | category | flops | bytes accessed | tf_op | source)
XLA Modules:
  0.0 99.3 jit_solution(17918516349640316193)
XLA Ops:
  0.6 1.4 %copy.24.q_ref = bf16[128,64]{1,0:T(8,128)(2,1)} copy(bf16[128,64]{0,1:T(8,128)(2,1)} %param.23) | data formatting | bytes 32768 | tf_op args[9]
  2.1 1.4 %copy.25.k_ref = bf16[128,64]{1,0:T(8,128)(2,1)} copy(bf16[128,64]{0,1:T(8,128)(2,1)} %param.24) | data formatting | bytes 32768 | tf_op args[10]
  3.5 1.4 %copy.22.route_ref = s32[128,2]{1,0:T(8,128)} copy(s32[128,2]{0,1:T(2,128)} %param.16) | data formatting | bytes 2048 | tf_op args[2]
  4.9 1.4 %copy.23.weight_ref = f32[128,2]{1,0:T(8,128)} copy(f32[128,2]{0,1:T(2,128)} %param.17) | data formatting | bytes 2048 | tf_op args[3]
  6.3 1.5 %copy.26.log_ref = f32[128,64]{1,0:T(8,128)} copy(f32[128,64]{0,1:T(8,128)} %param.26) | data formatting | bytes 65536 | tf_op args[12]
  7.8 74.1 %experts_and_attention.1 = (bf16[16,16,64,128]{3,2,1,0:T(8,128)(2,1)}, bf16[512,384]{1,0:T(8,128)(2,1)}, bf16[512,384]{1,0:T(8,128)(2,1)}, bf16[512,384]{1,0:T(8...) custom-call(s32[128,2]{1,0:T(8,128)} %copy.22.route_ref, ...), custom_call_target="tpu_custom_call" | custom-call | tf_op jit(solution)/shard_map/experts_and_attention/pallas_call | solution.py:515
  81.9 0.0 copy-start
  81.9 2.2 %copy-done = bf16[16,16,64,128]{3,2,1,0:T(8,128)(2,1)S(1)} copy-done((bf16[16,16,64,128]{3,2,1,0:T(8,128)(2,1)S(1)}, bf16[16,16,64,128]{3,2,1,0:T(8,128)(2,1)}, u32[]{:S(2)}) %copy-start) | copy-done | bytes 4194328
  84.1 0.0 copy-start.1
  84.1 1.0 %copy-done.1 = bf16[512,384]{1,0:T(8,128)(2,1)S(1)} copy-done((bf16[512,384]{1,0:T(8,128)(2,1)S(1)}, bf16[512,384]{1,0:T(8,128)(2,1)}, u32[]{:S(2)}) %copy-start.1) | copy-done | bytes 393240
  85.1 0.0 copy-start.2
  85.1 1.0 %copy-done.2 = bf16[512,384]{1,0:T(8,128)(2,1)S(1)} copy-done((bf16[512,384]{1,0:T(8,128)(2,1)S(1)}, bf16[512,384]{1,0:T(8,128)(2,1)}, u32[]{:S(2)}) %copy-start.2) | copy-done | bytes 393240
  86.1 0.0 copy-start.3
  86.1 1.0 %copy-done.3 = bf16[512,384]{1,0:T(8,128)(2,1)S(1)} copy-done((bf16[512,384]{1,0:T(8,128)(2,1)S(1)}, bf16[512,384]{1,0:T(8,128)(2,1)}, u32[]{:S(2)}) %copy-start.3) | copy-done | bytes 393240
  87.1 0.0 copy-start.4
  87.1 0.8 copy-done.4
  87.9 0.0 copy-start.5
  87.9 0.8 copy-done.5
  88.8 0.0 copy-start.6
  88.8 0.8 copy-done.6
  89.5 0.0 copy-start.7
  89.5 0.8 copy-done.7
  90.3 0.0 copy-start.8
  90.3 0.8 copy-done.8
  91.0 6.1 %weight_grads.1 = (bf16[1,2048,384]{2,1,0:T(8,128)(2,1)}, bf16[1,2048,384]{2,1,0:T(8,128)(2,1)}, bf16[1,384,2048]{2,1,0:T(8,128)(2,1)}, f32[128,128]{1,0:T(8,128...) custom-call(bf16[16,16,64,128]{3,2,1,0:T(8,128)(2,1)S(1)} %copy-done, ...), custom_call_target="tpu_custom_call" | custom-call | tf_op jit(solution)/shard_map/weight_grads/pallas_call | solution.py:544
  97.2 0.7 copy.27
  97.9 0.7 copy.28
  98.6 0.7 copy.29
Async XLA Ops:
  81.9 2.2 %copy-start = (bf16[16,16,64,128]{3,2,1,0:T(8,128)(2,1)S(1)}, bf16[16,16,64,128]{3,2,1,0:T(8,128)(2,1)}, u32[]{:S(2)}) copy-start(bf16[16,16,64,128]{3,2,1,0:T(8,128)(2,1)} %get-tuple-element.17.rows) | copy-start | bytes 12582916
  84.1 1.0 %copy-start.1 = (bf16[512,384]{1,0:T(8,128)(2,1)S(1)}, bf16[512,384]{1,0:T(8,128)(2,1)}, u32[]{:S(2)}) copy-start(bf16[512,384]{1,0:T(8,128)(2,1)} %get-tuple-element.18.hid) | copy-start | bytes 1179652
  85.1 1.0 %copy-start.2 = (bf16[512,384]{1,0:T(8,128)(2,1)S(1)}, bf16[512,384]{1,0:T(8,128)(2,1)}, u32[]{:S(2)}) copy-start(bf16[512,384]{1,0:T(8,128)(2,1)} %get-tuple-element.19.dg) | copy-start | bytes 1179652
  86.1 1.0 %copy-start.3 = (bf16[512,384]{1,0:T(8,128)(2,1)S(1)}, bf16[512,384]{1,0:T(8,128)(2,1)}, u32[]{:S(2)}) copy-start(bf16[512,384]{1,0:T(8,128)(2,1)} %get-tuple-element.20.du) | copy-start | bytes 1179652
  87.1 0.8 copy-start.4
  87.9 0.8 copy-start.5
  88.8 0.8 copy-start.6
  89.5 0.8 copy-start.7
  90.3 0.8 copy-start.8

commit v3 on v2

v3 whole, which is shorter than its diff:
```python
import functools

import jax
import jax.numpy as jnp
from jax import lax
from jax.experimental import pallas as pl
from jax.experimental.pallas import tpu as pltpu
from jax.sharding import PartitionSpec as P

BF = jnp.bfloat16
F32 = jnp.float32
HIGH = lax.Precision.HIGHEST
LANE = 128
DK = 64
SPAN = 64
NN = (((1,), (0,)), ((), ()))
NT = (((1,), (1,)), ((), ()))
TN = (((0,), (0,)), ((), ()))


def mm(a, b, dims=NN, precision=None):
    return lax.dot_general(a, b, dims, precision=precision, preferred_element_type=F32)


def half_dot(a, b, dims=NN):
    return mm(a.astype(BF), b.astype(BF), dims)


def waited(ref, sem):
    pltpu.make_async_copy(ref, ref, sem).wait()


def main_kernel(
    route_hbm, weight_hbm, input_hbm, cot_hbm, proj_hbm, saved_hbm, q_hbm, k_hbm, v_hbm, log_hbm,
    state_hbm, wg_hbm, wu_hbm, wd_hbm,
    gg_ref, gu_ref, gw_ref, gproj_ref, gq_ref, gk_ref, gv_ref, gd_ref,
    route_ref, weight_ref, input_ref, cot_ref, proj_ref, saved_ref, q_ref, k_ref, v_ref, log_ref,
    state_ref, wgu, wd, rows, hid_t, dgu, table, picks, send, gu_acc, hid_acc, tmp, mine, pair_out,
    pair_in, near_out, near_in, back_out, back_in, far_out, far_in, grad_in, all_in, all_saved,
    tot_out, tot_in,
    carry_out, carry_in, after,
    w_sem, load_sem, disp_s, disp_r, ring_s, ring_r, core_s, core_r, pair_s, pair_r, near_s, near_r, back_s, back_r,
    far_s, far_r, all_s, all_r, fwd_s, fwd_r, save_s, save_r, opp_s, opp_r, mate_s, mate_r, pj_s, pj_r, tot_s, tot_r, carry_s, carry_r,
    *, groups, lanes, capacity,
):
    chips = lanes // 2
    sp, tp = lax.axis_index("sp"), lax.axis_index("tp")
    z, core = lax.div(tp, 2), lax.rem(tp, 2)
    other = 1 - core
    tokens = input_ref.shape[0]
    slots = groups * capacity
    hidden = wd.shape[0]
    half = groups // 2

    def wrapped(rel):
        return lax.rem(z + rel, chips)

    def to(src, dst, send_sem, recv_sem, **where):
        pltpu.make_async_remote_copy(
            src_ref=src, dst_ref=dst, send_sem=send_sem, recv_sem=recv_sem,
            device_id=where, device_id_type=pl.DeviceIdType.MESH,
        ).start()

    def to_tp(src, dst, send_sem, recv_sem, chip, at_core):
        to(src, dst, send_sem, recv_sem, tp=chip * 2 + at_core)

    barrier = pltpu.get_barrier_semaphore()

    @pl.loop(1, groups)
    def _(o):
        pl.semaphore_signal(
            barrier, inc=1, device_id={"sp": lax.rem(sp + o, groups)},
            device_id_type=pl.DeviceIdType.MESH,
        )

    @pl.loop(1, chips)
    def _(o):
        pl.semaphore_signal(
            barrier, inc=1, device_id={"tp": wrapped(o) * 2 + core},
            device_id_type=pl.DeviceIdType.MESH,
        )

    pl.semaphore_signal(
        barrier, inc=1, device_id={"tp": z * 2 + other}, device_id_type=pl.DeviceIdType.MESH
    )

    given = [
        route_hbm, weight_hbm, input_hbm, cot_hbm, log_hbm, proj_hbm, saved_hbm, q_hbm, k_hbm,
        v_hbm, state_hbm,
    ]
    held = [
        route_ref, weight_ref, input_ref, cot_ref, log_ref, proj_ref, saved_ref, q_ref, k_ref,
        v_ref, state_ref,
    ]
    loads = [
        pltpu.make_async_copy(src, dst, load_sem.at[n])
        for n, (src, dst) in enumerate(zip(given, held))
    ]
    for copy in loads[:5]:
        copy.start()
    copies = [
        pltpu.make_async_copy(wg_hbm.at[0], wgu.at[:, pl.ds(0, hidden)], w_sem.at[0]),
        pltpu.make_async_copy(wu_hbm.at[0], wgu.at[:, pl.ds(hidden, hidden)], w_sem.at[1]),
        pltpu.make_async_copy(wd_hbm.at[0], wd, w_sem.at[2]),
    ]
    for copy in loads[:2]:
        copy.wait()
    experts = lax.broadcasted_iota(jnp.int32, (groups, tokens), 0)
    named = [(route_ref[j : j + 1, :] == experts).astype(F32) for j in (0, 1)]
    row = lax.broadcasted_iota(jnp.int32, (tokens, tokens), 0)
    col = lax.broadcasted_iota(jnp.int32, (tokens, tokens), 1)
    earlier = half_dot(named[0] + named[1], (row < col).astype(F32))
    place_in = lax.broadcasted_iota(jnp.int32, (slots, tokens), 0)
    found = []
    for j in (0, 1):
        place = jnp.sum(earlier * named[j], axis=0, keepdims=True).astype(jnp.int32)
        slot = route_ref[j : j + 1, :] * capacity + place
        found.append((slot == place_in).astype(F32))
        table[:, j * tokens : (j + 1) * tokens] = found[j].astype(BF)
    picks[...] = jnp.transpose(found[0] + found[1]).astype(BF)
    weights = jnp.transpose(
        jnp.concatenate([weight_ref[...], jnp.zeros((6, tokens), F32)], axis=0)
    )
    far_blocks = list(range(3, chips - 2)) if chips > 4 else [2]
    near = 2 if chips > 4 else 1
    firsts = [0] + far_blocks

    def fill(b, rel):
        t = wrapped(rel) * 2 + core
        columns = pl.ds(pl.multiple_of(t * LANE, LANE), LANE)
        cot = cot_ref[:, columns].astype(F32)
        ours = input_ref[:, columns]
        ins = mm(table[...], jnp.concatenate([ours, ours], axis=0))
        weighted = [(weights[:, j : j + 1] * cot).astype(BF) for j in (0, 1)]
        cots = mm(table[...], jnp.concatenate(weighted, axis=0))
        send[b, :, :capacity] = ins.astype(BF).reshape(groups, capacity, LANE)
        send[b, :, capacity:] = cots.astype(BF).reshape(groups, capacity, LANE)
        rows[t, sp] = send[b, sp]

    def dispatch(b, rel):
        t = wrapped(rel) * 2 + core

        @pl.loop(1, groups)
        def _(o):
            peer = lax.rem(sp + o, groups)
            to(send.at[b, peer], rows.at[t, sp], disp_s.at[b], disp_r.at[b], sp=peer)

    for copy in loads[2:5]:
        copy.wait()
    for copy in [*loads[5:], *copies]:
        copy.start()
    fill(0, 0)
    totals = mm(jnp.ones((8, tokens), F32), log_ref[...], NT, HIGH)
    tot_out[...] = jnp.concatenate(
        [totals, jnp.zeros((8, LANE - DK), F32)], axis=1
    )
    tot_in[sp] = tot_out[...]
    pl.semaphore_wait(barrier, groups - 1 + chips)

    dispatch(0, 0)
    for b, rel in enumerate(firsts):
        if b:
            fill(b, rel)
            dispatch(b, rel)

    @pl.loop(1, groups)
    def _(o):
        peer = lax.rem(sp + o, groups)
        to(tot_out, tot_in.at[sp], tot_s, tot_r, sp=peer)

    for copy in loads[5:]:
        copy.wait()

    @pl.loop(1, groups)
    def _(o):
        peer = lax.rem(sp + o, groups)
        to(saved_ref, all_saved.at[sp], save_s, save_r, sp=peer)

    all_saved[sp] = saved_ref[...]
    gu_acc[...] = jnp.zeros_like(gu_acc)
    hid_acc[...] = jnp.zeros_like(hid_acc)

    def halves(t, h):
        return rows.at[t, pl.ds(h * half, half)]

    def block(rel):
        return wrapped(rel) * 2 + core

    def pass_ring(rel, step, h, side):
        chip = wrapped(1 if side == 0 else chips - 1)
        part = halves(block(rel), h)
        to_tp(part, part, ring_s.at[step, side, h], ring_r.at[step, side, h], chip, core)

    def await_ring(rel, step, h, side):
        waited(halves(block(rel), h), ring_r.at[step, side, h])

    def to_other(rel):
        t = block(rel)
        to_tp(rows.at[t], rows.at[t], core_s.at[rel], core_r.at[rel], z, other)

    def from_other(rel):
        waited(rows.at[wrapped(rel) * 2 + other], core_r.at[rel])

    def both(zz, start):
        pieces = [
            rows[zz * 2 + k, :, start : start + capacity].reshape(slots, LANE) for k in (0, 1)
        ]
        return jnp.concatenate(pieces, axis=1)

    def gather_product(rel):
        zz = wrapped(rel)
        depth = pl.ds(pl.multiple_of(zz * 2 * LANE, 2 * LANE), 2 * LANE)
        ins = both(zz, 0)
        gu_acc[...] += mm(ins, wgu[depth, :])
        hid_acc[...] += mm(both(zz, capacity), wd[:, depth], NT)

    def await_dispatch(b):
        waited(send.at[b, pl.ds(0, groups - 1)], disp_r.at[b])

    def drain(phase):
        if phase >= 2:
            for b in range(len(firsts)):
                waited(send.at[b, pl.ds(0, groups - 1)], disp_s.at[b])
            waited(tot_in.at[pl.ds(0, groups - 1)], tot_s)
            waited(all_saved.at[pl.ds(0, groups - 1)], save_s)
        if phase >= 3:
            for step in range(near):
                for side in (0, 1):
                    for h in (0, 1):
                        waited(halves(0, h), ring_s.at[step, side, h])
            for rel in range(chips):
                waited(rows.at[0], core_s.at[rel])
        if phase >= 4:
            for j in range(chips):
                waited(pair_out.at[j], pair_s.at[j])
                if j < 2:
                    waited(near_out.at[j], near_s.at[j])
                else:
                    waited(back_out.at[j, pl.ds(0, groups - 1)], back_s.at[j])
                if 2 <= j < chips - 1:
                    waited(far_out.at[j], far_s.at[j])
        if phase >= 5:
            for rel in range(chips):
                waited(grad_in.at[0], fwd_s.at[rel])
                if rel not in (0, chips // 2):
                    waited(grad_in.at[0], all_s.at[rel])
            for side in (0, 1):
                waited(grad_in.at[0, pl.ds(0, tokens // 2)], opp_s.at[side])
        if phase >= 6:
            @pl.when(lax.rem(sp, 2) == core)
            def _():
                waited(all_in.at[pl.ds(0, chips - 1)], pj_s)
                waited(all_in, mate_s)

            @pl.when(lax.rem(sp, 2) != core)
            def _():
                waited(all_in.at[pl.ds(0, chips)], pj_s)

            for r in range(groups - 1):
                @pl.when(sp > r)
                def _():
                    waited(carry_out.at[r], carry_s.at[r])

    await_dispatch(0)
    for h in (0, 1):
        for side in (0, 1):
            pass_ring(0, 0, h, side)
    to_other(0)
    for copy in copies:
        copy.wait()
    from_other(0)
    gather_product(0)
    for h in (0, 1):
        for side in (0, 1):
            rel = chips - 1 if side == 0 else 1
            await_ring(rel, 0, h, side)
            if near > 1:
                pass_ring(rel, 1, h, side)
        if h == 0 and len(firsts) > 1:
            await_dispatch(1)
            to_other(firsts[1])
    to_other(1)
    to_other(chips - 1)
    for b, rel in enumerate(firsts):
        if b > 1:
            await_dispatch(b)
            to_other(rel)

    @pl.loop(0, len(far_blocks))
    def _(i):
        rel = far_blocks[0] + i
        from_other(rel)
        gather_product(rel)

    @pl.loop(0, 2)
    def _(i):
        rel = 1 + i * (chips - 2)
        from_other(rel)
        gather_product(rel)

    if near > 1:
        for side in (0, 1):
            rel = chips - 2 if side == 0 else 2
            for h in (0, 1):
                await_ring(rel, 1, h, side)
            to_other(rel)

        @pl.loop(0, 2)
        def _(i):
            rel = chips - 2 - i * (chips - 4)
            from_other(rel)
            gather_product(rel)

    tile = LANE

    @pl.loop(0, slots // tile)
    def _(i):
        at = pl.ds(pl.multiple_of(i * tile, tile), tile)
        gate = gu_acc[at, :hidden]
        upper = gu_acc[at, hidden:]
        d_hidden = hid_acc[at, :]
        sigmoid = jax.nn.sigmoid(gate)
        active = gate * sigmoid
        hid_t[:, at] = jnp.transpose(active * upper).astype(BF)
        dgu[at, hidden:] = (d_hidden * active).astype(BF)
        dgu[at, :hidden] = (
            d_hidden * upper * sigmoid * (1.0 + gate * (1.0 - sigmoid))
        ).astype(BF)

    def turn(j):
        far = chips // 2 + lax.div(j - 1, 2) * (2 * lax.rem(j, 2) - 1)
        rel = jnp.where(j < 2, 1 + j * (chips - 2), jnp.where(j == chips - 1, 0, far))
        return rel

    def slot_block(j):
        zz = wrapped(turn(j))
        depth = pl.ds(pl.multiple_of(zz * 2 * LANE, 2 * LANE), 2 * LANE)
        tmp[...] = mm(dgu[...], wgu[depth, :], NT)
        pair_out[j] = tmp[:, pl.ds(pl.multiple_of(other * LANE, LANE), LANE)].astype(BF)
        mine[j] = tmp[:, pl.ds(pl.multiple_of(core * LANE, LANE), LANE)]
        to_tp(pair_out.at[j], pair_in.at[j], pair_s.at[j], pair_r.at[j], z, other)

    def slot_near(j):
        waited(pair_in.at[j], pair_r.at[j])
        near_out[j] = (mine[j] + pair_in[j].astype(F32)).astype(BF)
        to_tp(
            near_out.at[j], near_in.at[j], near_s.at[j], near_r.at[j], wrapped(turn(j)), core
        )

    def slot_send(j, whole):
        back_out[j] = whole.astype(BF).reshape(groups, capacity, LANE)
        back_in[j, sp] = back_out[j, sp]

        @pl.loop(1, groups)
        def _(o):
            peer = lax.rem(sp + o, groups)
            to(back_out.at[j, peer], back_in.at[j, sp], back_s.at[j], back_r.at[j], sp=peer)

    def slot_return(j):
        waited(pair_in.at[j], pair_r.at[j])
        slot_send(j, mine[j] + pair_in[j].astype(F32))

    lag = 2

    @pl.loop(0, chips + lag - 1)
    def _(j):
        @pl.when(j < chips)
        def _():
            slot_block(j)

        @pl.when((j >= lag) & (j < 2 * lag))
        def _():
            slot_near(j - lag)

        @pl.when(j >= 2 * lag)
        def _():
            slot_return(j - lag)

    def weight_block(zz):
        depth = pl.ds(pl.multiple_of(zz * 2 * LANE, 2 * LANE), 2 * LANE)
        pair = mm(both(zz, 0), dgu[...], TN).astype(BF)
        gg_ref[depth, :] = pair[:, :hidden]
        gu_ref[depth, :] = pair[:, hidden:]
        gw_ref[:, depth] = mm(hid_t[...], both(zz, capacity)).astype(BF)

    weight_block(0)
    weight_block(1)
    own = chips - 1
    waited(pair_in.at[own], pair_r.at[own])
    summed = mine[own] + pair_in[own].astype(F32)
    for j in (0, 1):
        waited(near_in.at[j], near_r.at[j])
        summed += near_in[j].astype(F32)
    slot_send(own, summed)

    def routed(j):
        waited(back_out.at[j, pl.ds(0, groups - 1)], back_r.at[j])
        return mm(picks[...], back_in[j].reshape(slots, LANE))

    @pl.loop(2, chips - 1)
    def _(j):
        rel = turn(j)
        far_out[j] = routed(j).astype(BF)
        to_tp(far_out.at[j], far_in.at[rel], far_s.at[j], far_r.at[rel], wrapped(rel), core)
        weight_block(j)

    weight_block(chips - 1)
    total = routed(chips - 1)
    same_span = lax.div(row, SPAN) == lax.div(col, SPAN)
    causal = (row >= col) & same_span
    until = ((row <= col) & same_span).astype(F32)
    since = causal.astype(F32)
    cum = mm(log_ref[...], until, NN, HIGH)
    waited(tot_in.at[pl.ds(0, groups - 1)], tot_r)
    after_row = lax.broadcasted_iota(jnp.int32, (groups, LANE), 0)
    after_col = lax.broadcasted_iota(jnp.int32, (groups, LANE), 1)
    between = ((after_row > after_col) & (after_row < sp)).astype(F32)
    factors = jnp.exp(mm(tot_in[:, 0, :DK], between, TN, HIGH))

    for rel in range(2, chips - 1):
        waited(far_in.at[rel], far_r.at[rel])
        total += far_in[rel].astype(F32)
    columns = pl.ds(pl.multiple_of(tp * LANE, LANE), LANE)
    grad_in[tp] = (cot_ref[:, columns].astype(F32) + total).astype(BF)
    reach = chips // 2 - 1
    order = [r for k in range(reach, 0, -1) for r in (k, chips - k)]
    for rel in order:
        to_tp(grad_in.at[tp], grad_in.at[tp], all_s.at[rel], all_r.at[rel], wrapped(rel), core)
    to_tp(grad_in.at[tp], grad_in.at[tp], fwd_s.at[0], fwd_r.at[0], z, other)

    def to_owner(t):
        @pl.when(t != sp)
        def _():
            to(grad_in.at[t], all_in.at[sp], pj_s, pj_r, sp=t)

        @pl.when(t == sp)
        def _():
            all_in[sp] = grad_in[t]

    def to_pair(rel, t):
        to_tp(grad_in.at[t], grad_in.at[t], fwd_s.at[rel], fwd_r.at[rel], z, other)

    half_rows = tokens // 2
    to_owner(tp)
    for rel in order:
        t = wrapped(chips - rel) * 2 + core
        waited(grad_in.at[t], all_r.at[rel])
        if rel in (reach, chips - reach):
            side = 0 if rel == reach else 1
            part = grad_in.at[t, pl.ds(side * half_rows, half_rows)]
            chip = wrapped(1 if side == 0 else chips - 1)
            to_tp(part, part, opp_s.at[side], opp_r.at[side], chip, core)
        to_pair(rel, t)
        to_owner(t)
    t = wrapped(chips // 2) * 2 + core
    for side in (0, 1):
        waited(grad_in.at[t, pl.ds(0, half_rows)], opp_r.at[side])
    to_pair(chips // 2, t)
    to_owner(t)
    for rel in [0, *order, chips // 2]:
        t = wrapped(chips - rel if rel else 0) * 2 + other
        waited(grad_in.at[t], fwd_r.at[rel])

    mix = jnp.zeros((tokens, LANE), F32)
    for zz in range(chips):
        pair = jnp.concatenate([grad_in[2 * zz], grad_in[2 * zz + 1]], axis=1)
        mix += mm(pair, proj_ref[:, 2 * zz * LANE : 2 * (zz + 1) * LANE], NT)

    scale = DK ** (-0.5)
    grown = jnp.exp(cum)
    shrunk = jnp.exp(-cum)
    queries = q_ref[...].astype(F32)
    keys = k_ref[...].astype(F32)
    qd = (queries * grown).astype(BF)
    kd = (keys * shrunk).astype(BF)
    mix_half = mix.astype(BF)
    spans = [slice(n * SPAN, (n + 1) * SPAN) for n in (0, 1)]
    local = [scale * mm(qd[:, s], mix_half[s]) for s in spans]
    ends = [cum[:, (n + 1) * SPAN - 1 : (n + 1) * SPAN] for n in (0, 1)]
    last = [jnp.exp(e) for e in ends]
    begin = local[0] + last[0] * local[1]
    for r in range(groups - 1):
        @pl.when(sp > r)
        def _():
            carry_out[r] = (begin * factors[:, r : r + 1]).astype(BF)
            to(carry_out.at[r], carry_in.at[sp], carry_s.at[r], carry_r.at[sp], sp=r)

    values = v_ref[...]
    to_end = jnp.concatenate([jnp.exp(ends[n] - cum[:, spans[n]]) for n in (0, 1)], axis=1)
    ke = (keys * to_end).astype(BF)
    scores = jnp.where(causal, mm(qd, kd, TN), 0.0).astype(BF)
    dots = jnp.where(causal, mm(mix_half, values, NT), 0.0).astype(BF)
    from_state = jnp.concatenate(
        [mm(state_ref[n].astype(BF), mix_half[spans[n]], NT) for n in (0, 1)], axis=1
    )
    dq = scale * grown * (mm(kd, dots, NT) + from_state)
    dk = scale * shrunk * mm(qd, dots)
    dv = scale * mm(scores, mix_half, TN)
    state_end = [last[n] * state_ref[n] + mm(ke[:, spans[n]], values[spans[n]]) for n in (0, 1)]
    gq_ref[...] = dq.astype(BF)

    mate = lax.rem(sp, 2) == core

    @pl.when(mate)
    def _():
        waited(all_in.at[pl.ds(0, groups - 1)], pj_r)
        to_tp(all_in, all_in, mate_s, mate_r, z, other)

    after[...] = jnp.zeros_like(after)
    for s in range(1, groups):
        @pl.when(s > sp)
        def _():
            waited(carry_in.at[s], carry_r.at[s])
            after[...] += carry_in[s].astype(F32)

    end_1 = after[...]
    g_end = [local[1] + last[1] * end_1, end_1]
    half_end = [g.astype(BF) for g in g_end]
    dk = dk + to_end * jnp.concatenate(
        [mm(half_end[n], values[spans[n]], NT) for n in (0, 1)], axis=1
    )
    dv = dv + jnp.concatenate([mm(ke[:, spans[n]], half_end[n], TN) for n in (0, 1)], axis=0)
    tails = [jnp.sum(state_end[n] * g_end[n], axis=1, keepdims=True) for n in (0, 1)]
    tail = jnp.concatenate([jnp.broadcast_to(t, (DK, SPAN)) for t in tails], axis=1)
    gd_ref[...] = mm(queries * dq - keys * dk, since, NN, HIGH) + tail
    gk_ref[...] = dk.astype(BF)
    gv_ref[...] = dv.astype(BF)

    @pl.when(jnp.logical_not(mate))
    def _():
        waited(all_in, mate_r)

    waited(all_saved.at[pl.ds(0, groups - 1)], save_r)
    depth = groups * tokens
    gproj_ref[...] = mm(
        all_in[...].reshape(depth, LANE), all_saved[...].reshape(depth, LANE), TN
    )
    drain(6)


def store_kernel(*refs):
    count = (len(refs) - 1) // 2
    sems = refs[-1]
    copies = []
    for n, (src, dst) in enumerate(zip(refs[:count], refs[count : 2 * count])):
        copy = pltpu.make_async_copy(src, dst.at[0] if len(dst.shape) > 2 else dst, sems.at[n])
        copy.start()
        copies.append(copy)
    for copy in copies:
        copy.wait()


def on_device(
    moe_input, cotangent, route_expert, route_weight, w_gate, w_up, w_down, out_proj, saved_out,
    queries, keys, values, log_decay, span_state,
):
    groups, lanes = lax.axis_size("sp"), lax.axis_size("tp")
    tokens, width = moe_input.shape
    capacity = 4 * tokens // groups
    slots = groups * capacity
    hidden = w_gate.shape[2]
    chips = lanes // 2
    firsts = 4 if chips > 4 else 2
    vmem = pl.BlockSpec(memory_space=pltpu.VMEM)
    hbm = pl.BlockSpec(memory_space=pltpu.HBM)
    dma = pltpu.SemaphoreType.DMA
    shape = jax.ShapeDtypeStruct
    slab = (groups, 2 * capacity, LANE)
    scratch = [
        pltpu.VMEM((2, tokens), jnp.int32),
        pltpu.VMEM((2, tokens), F32),
        pltpu.VMEM((tokens, width), BF),
        pltpu.VMEM((tokens, width), BF),
        pltpu.VMEM((LANE, width), BF),
        pltpu.VMEM((tokens, LANE), BF),
        pltpu.VMEM((DK, tokens), BF),
        pltpu.VMEM((DK, tokens), BF),
        pltpu.VMEM((tokens, LANE), BF),
        pltpu.VMEM((DK, tokens), F32),
        pltpu.VMEM((2, DK, LANE), F32),
        pltpu.VMEM((width, 2 * hidden), BF),
        pltpu.VMEM((hidden, width), BF),
        pltpu.VMEM((lanes, *slab), BF),
        pltpu.VMEM((hidden, slots), BF),
        pltpu.VMEM((slots, 2 * hidden), BF),
        pltpu.VMEM((slots, 2 * tokens), BF),
        pltpu.VMEM((tokens, slots), BF),
        pltpu.VMEM((firsts, *slab), BF),
        pltpu.VMEM((slots, 2 * hidden), F32),
        pltpu.VMEM((slots, hidden), F32),
        pltpu.VMEM((slots, 2 * LANE), F32),
        pltpu.VMEM((chips, slots, LANE), F32),
        pltpu.VMEM((chips, slots, LANE), BF),
        pltpu.VMEM((chips, slots, LANE), BF),
        pltpu.VMEM((2, slots, LANE), BF),
        pltpu.VMEM((2, slots, LANE), BF),
        pltpu.VMEM((chips, groups, capacity, LANE), BF),
        pltpu.VMEM((chips, groups, capacity, LANE), BF),
        pltpu.VMEM((chips, tokens, LANE), BF),
        pltpu.VMEM((chips, tokens, LANE), BF),
        pltpu.VMEM((lanes, tokens, LANE), BF),
        pltpu.VMEM((groups, tokens, LANE), BF),
        pltpu.VMEM((groups, tokens, LANE), BF),
        pltpu.VMEM((8, LANE), F32),
        pltpu.VMEM((groups, 8, LANE), F32),
        pltpu.VMEM((groups, DK, LANE), BF),
        pltpu.VMEM((groups, DK, LANE), BF),
        pltpu.VMEM((DK, LANE), F32),
        dma((3,)), dma((11,)),
        dma((firsts,)), dma((firsts,)),
        dma((2, 2, 2)), dma((2, 2, 2)),
        dma((chips,)), dma((chips,)),
        dma((chips,)), dma((chips,)),
        dma((2,)), dma((2,)),
        dma((chips,)), dma((chips,)),
        dma((chips,)), dma((chips,)),
        dma((chips,)), dma((chips,)),
        dma((chips,)), dma((chips,)),
        dma, dma, dma((2,)), dma((2,)), dma, dma,
        dma, dma, dma, dma,
        dma((groups,)), dma((groups,)),
    ]
    made = (
        pltpu.VMEM((width, hidden), BF),
        pltpu.VMEM((width, hidden), BF),
        pltpu.VMEM((hidden, width), BF),
        pltpu.VMEM((LANE, LANE), F32),
        pltpu.VMEM((DK, tokens), BF),
        pltpu.VMEM((DK, tokens), BF),
        pltpu.VMEM((tokens, LANE), BF),
        pltpu.VMEM((DK, tokens), F32),
    )
    results = pl.pallas_call(
        functools.partial(main_kernel, groups=groups, lanes=lanes, capacity=capacity),
        name="experts_and_attention",
        out_shape=made,
        in_specs=[hbm] * 14,
        out_specs=(vmem,) * 8,
        scratch_shapes=scratch,
        compiler_params=pltpu.CompilerParams(
            collective_id=0, has_side_effects=True, vmem_limit_bytes=62105600
        ),
    )(
        route_expert.T, route_weight.T, moe_input, cotangent, out_proj, saved_out, queries.T,
        keys.T, values, log_decay.T, span_state, w_gate, w_up, w_down,
    )
    results = pl.pallas_call(
        store_kernel,
        name="store_results",
        out_shape=tuple(
            shape((1, *a.shape) if n < 3 else a.shape, a.dtype) for n, a in enumerate(results)
        ),
        in_specs=[vmem] * 8,
        out_specs=(hbm,) * 8,
        scratch_shapes=[dma((8,))],
        compiler_params=pltpu.CompilerParams(vmem_limit_bytes=1024 * 1024),
    )(*(pltpu.with_memory_space_constraint(r, pltpu.VMEM) for r in results))
    gg, gu, gw, gp, gq, gk, gv, gd = results
    return gg, gu, gw, gp, gq.T, gk.T, gv, gd.T


def solution(mesh):
    placed = (
        P("sp", None),
        P("sp", None),
        P("sp", None),
        P("sp", None),
        P("sp", None, "tp"),
        P("sp", None, "tp"),
        P("sp", "tp", None),
        P("tp", None),
        P("sp", "tp"),
        P("sp", "tp"),
        P("sp", "tp"),
        P("sp", "tp"),
        P("sp", "tp"),
        P("sp", "tp", None),
    )
    return jax.shard_map(
        on_device,
        mesh=mesh,
        in_specs=placed,
        out_specs=(
            P("sp", None, "tp"),
            P("sp", None, "tp"),
            P("sp", "tp", None),
            P("sp", "tp"),
            P("sp", "tp"),
            P("sp", "tp"),
            P("sp", "tp"),
            P("sp", "tp"),
        ),
        check_vma=False,
    )
```

time: 100 us -> 71.7 us (0.72)
  local copies, waits for them, and re-layouts: 18.4 us -> 0 us
  Pallas kernels: 80.2 us -> 70.9 us
    unnamed x23 -> x0, local copies, waits for them, and re-layouts: 16.3 us -> none
    pallas_call x1, Pallas kernels: 74.1 us -> 68.6 us  [on_device(): pl.pallas_call(functools.partial(main_kernel, groups=groups, lanes=lanes,...]
    pallas_call x1, Pallas kernels: 6.13 us -> 2.28 us  [on_device(): pl.pallas_call(store_kernel, name='store_results', out_shape=tuple((shape...]
    pallas_call x3 -> x0, local copies, waits for them, and re-layouts: 2.09 us -> none  [on_device(): pl.pallas_call(weight_kernel, name='weight_grads', grid=(chips,), out_sha...]
where the time goes in v3:
time: 71.7 us; the launch traced here: 71.6 us
  Pallas kernels  70.9 us (99%)
    pallas_call x1, Pallas kernels, on_device(): pl.pallas_call(functools.partial(main_kernel, groups=groups, lanes=lanes,...  68.6 us
    pallas_call x1, Pallas kernels, on_device(): pl.pallas_call(store_kernel, name='store_results', out_shape=tuple((shape...  2.28 us

profile of v3, /device:TPU:1, one launch (start us, length us, event | category | flops | bytes accessed | tf_op | source)
XLA Modules:
  0.0 71.6 jit_solution(1123577094782087912)
XLA Ops:
  0.6 68.6 %experts_and_attention.1 = (bf16[2048,384]{1,0:T(8,128)(2,1)S(1)}, bf16[2048,384]{1,0:T(8,128)(2,1)S(1)}, bf16[384,2048]{1,0:T(8,128)(2,1)S(1)}, f32[128,128]{1,...) custom-call(s32[2,128]{1,0:T(2,128)} %bitcast.11, ...), custom_call_target="tpu_custom_call" | custom-call | tf_op jit(solution)/shard_map/experts_and_attention/pallas_call | solution.py:633
  69.3 2.3 %store_results.1 = (bf16[1,2048,384]{2,1,0:T(8,128)(2,1)}, bf16[1,2048,384]{2,1,0:T(8,128)(2,1)}, bf16[1,384,2048]{2,1,0:T(8,128)(2,1)}, f32[128,128]{1,0:T(8,12...) custom-call(bf16[2048,384]{1,0:T(8,128)(2,1)S(1)} %get-tuple-element.24.re, ...), custom_call_target="tpu_custom_call" | custom-call | tf_op jit(solution)/shard_map/store_results/pallas_call | solution.py:647

commit v4 on v3

--- a/solution.py
+++ b/solution.py
@@ -39,7 +39,7 @@
     pair_in, near_out, near_in, back_out, back_in, far_out, far_in, grad_in, all_in, all_saved,
     tot_out, tot_in,
     carry_out, carry_in, after,
-    w_sem, load_sem, disp_s, disp_r, ring_s, ring_r, core_s, core_r, pair_s, pair_r, near_s, near_r, back_s, back_r,
+    w_sem, load_sem, disp_s, disp_r, ring_s, ring_r, core_s, core_r, late_s, late_r, pair_s, pair_r, near_s, near_r, back_s, back_r,
     far_s, far_r, all_s, all_r, fwd_s, fwd_r, save_s, save_r, opp_s, opp_r, mate_s, mate_r, pj_s, pj_r, tot_s, tot_r, carry_s, carry_r,
     *, groups, lanes, capacity,
 ):
@@ -50,7 +50,6 @@
     tokens = input_ref.shape[0]
     slots = groups * capacity
     hidden = wd.shape[0]
-    half = groups // 2
 
     def wrapped(rel):
         return lax.rem(z + rel, chips)
@@ -121,29 +120,34 @@
     weights = jnp.transpose(
         jnp.concatenate([weight_ref[...], jnp.zeros((6, tokens), F32)], axis=0)
     )
-    far_blocks = list(range(3, chips - 2)) if chips > 4 else [2]
-    near = 2 if chips > 4 else 1
-    firsts = [0] + far_blocks
+    far_blocks = range(3, chips - 2)
+    late = (2, chips - 2)
+    firsts = [0, *far_blocks, *late]
 
     def fill(b, rel):
         t = wrapped(rel) * 2 + core
         columns = pl.ds(pl.multiple_of(t * LANE, LANE), LANE)
+        if rel not in late:
+            ours = input_ref[:, columns]
+            ins = mm(table[...], jnp.concatenate([ours, ours], axis=0))
+            send[b, 0] = ins.astype(BF).reshape(groups, capacity, LANE)
+            rows[t, 0, sp] = send[b, 0, sp]
         cot = cot_ref[:, columns].astype(F32)
-        ours = input_ref[:, columns]
-        ins = mm(table[...], jnp.concatenate([ours, ours], axis=0))
         weighted = [(weights[:, j : j + 1] * cot).astype(BF) for j in (0, 1)]
         cots = mm(table[...], jnp.concatenate(weighted, axis=0))
-        send[b, :, :capacity] = ins.astype(BF).reshape(groups, capacity, LANE)
-        send[b, :, capacity:] = cots.astype(BF).reshape(groups, capacity, LANE)
-        rows[t, sp] = send[b, sp]
-
-    def dispatch(b, rel):
+        send[b, 1] = cots.astype(BF).reshape(groups, capacity, LANE)
+        rows[t, 1, sp] = send[b, 1, sp]
+
+    def dispatch(b, rel, p):
         t = wrapped(rel) * 2 + core
 
         @pl.loop(1, groups)
         def _(o):
             peer = lax.rem(sp + o, groups)
-            to(send.at[b, peer], rows.at[t, sp], disp_s.at[b], disp_r.at[b], sp=peer)
+            to(send.at[b, p, peer], rows.at[t, p, sp], disp_s.at[b, p], disp_r.at[b, p], sp=peer)
+
+    def pieces(rel):
+        return (1,) if rel in late else (0, 1)
 
     for copy in loads[2:5]:
         copy.wait()
@@ -157,11 +161,11 @@
     tot_in[sp] = tot_out[...]
     pl.semaphore_wait(barrier, groups - 1 + chips)
 
-    dispatch(0, 0)
     for b, rel in enumerate(firsts):
         if b:
             fill(b, rel)
-            dispatch(b, rel)
+        for p in pieces(rel):
+            dispatch(b, rel, p)
 
     @pl.loop(1, groups)
     def _(o):
@@ -170,29 +174,19 @@
 
     for copy in loads[5:]:
         copy.wait()
-
-    @pl.loop(1, groups)
-    def _(o):
-        peer = lax.rem(sp + o, groups)
-        to(saved_ref, all_saved.at[sp], save_s, save_r, sp=peer)
-
-    all_saved[sp] = saved_ref[...]
     gu_acc[...] = jnp.zeros_like(gu_acc)
     hid_acc[...] = jnp.zeros_like(hid_acc)
 
-    def halves(t, h):
-        return rows.at[t, pl.ds(h * half, half)]
-
     def block(rel):
         return wrapped(rel) * 2 + core
 
-    def pass_ring(rel, step, h, side):
+    def pass_ring(rel, step, p, side):
         chip = wrapped(1 if side == 0 else chips - 1)
-        part = halves(block(rel), h)
-        to_tp(part, part, ring_s.at[step, side, h], ring_r.at[step, side, h], chip, core)
-
-    def await_ring(rel, step, h, side):
-        waited(halves(block(rel), h), ring_r.at[step, side, h])
+        part = rows.at[block(rel), p]
+        to_tp(part, part, ring_s.at[step, side, p], ring_r.at[step, side, p], chip, core)
+
+    def await_ring(rel, step, p, side):
+        waited(rows.at[block(rel), p], ring_r.at[step, side, p])
 
     def to_other(rel):
         t = block(rel)
@@ -201,44 +195,52 @@
     def from_other(rel):
         waited(rows.at[wrapped(rel) * 2 + other], core_r.at[rel])
 
-    def both(zz, start):
-        pieces = [
-            rows[zz * 2 + k, :, start : start + capacity].reshape(slots, LANE) for k in (0, 1)
-        ]
-        return jnp.concatenate(pieces, axis=1)
+    def late_to_other(i, p):
+        part = rows.at[block(late[i]), p]
+        to_tp(part, part, late_s.at[i, p], late_r.at[i, p], z, other)
+
+    def both(zz, p):
+        return jnp.concatenate(
+            [rows[zz * 2 + k, p].reshape(slots, LANE) for k in (0, 1)], axis=1
+        )
+
+    def depth_of(zz):
+        return pl.ds(pl.multiple_of(zz * 2 * LANE, 2 * LANE), 2 * LANE)
 
     def gather_product(rel):
         zz = wrapped(rel)
-        depth = pl.ds(pl.multiple_of(zz * 2 * LANE, 2 * LANE), 2 * LANE)
-        ins = both(zz, 0)
-        gu_acc[...] += mm(ins, wgu[depth, :])
-        hid_acc[...] += mm(both(zz, capacity), wd[:, depth], NT)
-
-    def await_dispatch(b):
-        waited(send.at[b, pl.ds(0, groups - 1)], disp_r.at[b])
+        gu_acc[...] += mm(both(zz, 0), wgu[depth_of(zz), :])
+        hid_acc[...] += mm(both(zz, 1), wd[:, depth_of(zz)], NT)
+
+    def await_dispatch(b, p):
+        waited(send.at[b, p, pl.ds(0, groups - 1)], disp_r.at[b, p])
 
     def drain(phase):
         if phase >= 2:
-            for b in range(len(firsts)):
-                waited(send.at[b, pl.ds(0, groups - 1)], disp_s.at[b])
+            for b, rel in enumerate(firsts):
+                for p in pieces(rel):
+                    waited(send.at[b, p, pl.ds(0, groups - 1)], disp_s.at[b, p])
             waited(tot_in.at[pl.ds(0, groups - 1)], tot_s)
+        if phase >= 3:
+            for side in (0, 1):
+                waited(rows.at[0, 0], ring_s.at[0, side, 0])
+                waited(rows.at[0, 0], ring_s.at[0, side, 1])
+                waited(rows.at[0, 0], ring_s.at[1, side, 0])
+                for p in (0, 1):
+                    waited(rows.at[0, 0], late_s.at[side, p])
+            for rel in range(chips):
+                if rel not in late:
+                    waited(rows.at[0], core_s.at[rel])
+        if phase >= 4:
             waited(all_saved.at[pl.ds(0, groups - 1)], save_s)
-        if phase >= 3:
-            for step in range(near):
-                for side in (0, 1):
-                    for h in (0, 1):
-                        waited(halves(0, h), ring_s.at[step, side, h])
-            for rel in range(chips):
-                waited(rows.at[0], core_s.at[rel])
-        if phase >= 4:
             for j in range(chips):
                 waited(pair_out.at[j], pair_s.at[j])
-                if j < 2:
-                    waited(near_out.at[j], near_s.at[j])
+                if j in (2, 3):
+                    waited(near_out.at[j - 2], near_s.at[j - 2])
                 else:
                     waited(back_out.at[j, pl.ds(0, groups - 1)], back_s.at[j])
-                if 2 <= j < chips - 1:
-                    waited(far_out.at[j], far_s.at[j])
+                    if j < chips - 1:
+                        waited(far_out.at[j], far_s.at[j])
         if phase >= 5:
             for rel in range(chips):
                 waited(grad_in.at[0], fwd_s.at[rel])
@@ -261,36 +263,29 @@
                 def _():
                     waited(carry_out.at[r], carry_s.at[r])
 
-    await_dispatch(0)
-    for h in (0, 1):
+    for p in (0, 1):
+        await_dispatch(0, p)
         for side in (0, 1):
-            pass_ring(0, 0, h, side)
+            pass_ring(0, 0, p, side)
     to_other(0)
     for copy in copies:
         copy.wait()
     from_other(0)
     gather_product(0)
-    for h in (0, 1):
-        for side in (0, 1):
-            rel = chips - 1 if side == 0 else 1
-            await_ring(rel, 0, h, side)
-            if near > 1:
-                pass_ring(rel, 1, h, side)
-        if h == 0 and len(firsts) > 1:
-            await_dispatch(1)
-            to_other(firsts[1])
-    to_other(1)
-    to_other(chips - 1)
-    for b, rel in enumerate(firsts):
-        if b > 1:
-            await_dispatch(b)
-            to_other(rel)
-
-    @pl.loop(0, len(far_blocks))
-    def _(i):
-        rel = far_blocks[0] + i
-        from_other(rel)
-        gather_product(rel)
+    for side in (0, 1):
+        rel = chips - 1 if side == 0 else 1
+        await_ring(rel, 0, 0, side)
+        pass_ring(rel, 1, 0, side)
+    for p in (0, 1):
+        await_dispatch(1, p)
+    to_other(firsts[1])
+    for side in (0, 1):
+        rel = chips - 1 if side == 0 else 1
+        await_ring(rel, 0, 1, side)
+        to_other(rel)
+    for p in (0, 1):
+        await_dispatch(2, p)
+    to_other(firsts[2])
 
     @pl.loop(0, 2)
     def _(i):
@@ -298,18 +293,32 @@
         from_other(rel)
         gather_product(rel)
 
-    if near > 1:
-        for side in (0, 1):
-            rel = chips - 2 if side == 0 else 2
-            for h in (0, 1):
-                await_ring(rel, 1, h, side)
-            to_other(rel)
-
-        @pl.loop(0, 2)
-        def _(i):
-            rel = chips - 2 - i * (chips - 4)
-            from_other(rel)
-            gather_product(rel)
+    for p in (0, 1):
+        await_dispatch(3, p)
+    to_other(firsts[3])
+
+    @pl.loop(0, len(far_blocks) - 1)
+    def _(i):
+        rel = far_blocks[0] + i
+        from_other(rel)
+        gather_product(rel)
+
+    for i in (0, 1):
+        await_ring(late[i], 1, 0, 1 - i)
+        late_to_other(i, 0)
+    from_other(far_blocks[-1])
+    gather_product(far_blocks[-1])
+    for i in (0, 1):
+        await_dispatch(4 + i, 1)
+        late_to_other(i, 1)
+    for p in (0, 1):
+        for i in (0, 1):
+            zz = wrapped(late[i])
+            waited(rows.at[zz * 2 + other, p], late_r.at[i, p])
+            if p == 0:
+                gu_acc[...] += mm(both(zz, 0), wgu[depth_of(zz), :])
+            else:
+                hid_acc[...] += mm(both(zz, 1), wd[:, depth_of(zz)], NT)
 
     tile = LANE
 
@@ -328,9 +337,10 @@
         ).astype(BF)
 
     def turn(j):
-        far = chips // 2 + lax.div(j - 1, 2) * (2 * lax.rem(j, 2) - 1)
-        rel = jnp.where(j < 2, 1 + j * (chips - 2), jnp.where(j == chips - 1, 0, far))
-        return rel
+        k = jnp.where(j < 2, j, j - 2)
+        far = chips // 2 + lax.div(k + 1, 2) * (2 * lax.rem(k, 2) - 1)
+        near = 1 + (j - 2) * (chips - 2)
+        return jnp.where((j == 2) | (j == 3), near, jnp.where(j == chips - 1, 0, far))
 
     def slot_block(j):
         zz = wrapped(turn(j))
@@ -342,9 +352,11 @@
 
     def slot_near(j):
         waited(pair_in.at[j], pair_r.at[j])
-        near_out[j] = (mine[j] + pair_in[j].astype(F32)).astype(BF)
+        side = j - 2
+        near_out[side] = (mine[j] + pair_in[j].astype(F32)).astype(BF)
         to_tp(
-            near_out.at[j], near_in.at[j], near_s.at[j], near_r.at[j], wrapped(turn(j)), core
+            near_out.at[side], near_in.at[side], near_s.at[side], near_r.at[side],
+            wrapped(turn(j)), core,
         )
 
     def slot_send(j, whole):
@@ -368,20 +380,22 @@
         def _():
             slot_block(j)
 
-        @pl.when((j >= lag) & (j < 2 * lag))
+        i = j - lag
+
+        @pl.when((i == 2) | (i == 3))
         def _():
-            slot_near(j - lag)
-
-        @pl.when(j >= 2 * lag)
+            slot_near(i)
+
+        @pl.when((i >= 0) & (i != 2) & (i != 3))
         def _():
-            slot_return(j - lag)
+            slot_return(i)
 
     def weight_block(zz):
-        depth = pl.ds(pl.multiple_of(zz * 2 * LANE, 2 * LANE), 2 * LANE)
+        depth = depth_of(zz)
         pair = mm(both(zz, 0), dgu[...], TN).astype(BF)
         gg_ref[depth, :] = pair[:, :hidden]
         gu_ref[depth, :] = pair[:, hidden:]
-        gw_ref[:, depth] = mm(hid_t[...], both(zz, capacity)).astype(BF)
+        gw_ref[:, depth] = mm(hid_t[...], both(zz, 1)).astype(BF)
 
     weight_block(0)
     weight_block(1)
@@ -393,16 +407,24 @@
         summed += near_in[j].astype(F32)
     slot_send(own, summed)
 
+    @pl.loop(1, groups)
+    def _(o):
+        peer = lax.rem(sp + o, groups)
+        to(saved_ref, all_saved.at[sp], save_s, save_r, sp=peer)
+
+    all_saved[sp] = saved_ref[...]
+
     def routed(j):
         waited(back_out.at[j, pl.ds(0, groups - 1)], back_r.at[j])
         return mm(picks[...], back_in[j].reshape(slots, LANE))
 
-    @pl.loop(2, chips - 1)
-    def _(j):
+    @pl.loop(0, chips - 3)
+    def _(i):
+        j = jnp.where(i < 2, i, i + 2)
         rel = turn(j)
         far_out[j] = routed(j).astype(BF)
         to_tp(far_out.at[j], far_in.at[rel], far_s.at[j], far_r.at[rel], wrapped(rel), core)
-        weight_block(j)
+        weight_block(i + 2)
 
     weight_block(chips - 1)
     total = routed(chips - 1)
@@ -560,12 +582,12 @@
     slots = groups * capacity
     hidden = w_gate.shape[2]
     chips = lanes // 2
-    firsts = 4 if chips > 4 else 2
+    firsts = 6
     vmem = pl.BlockSpec(memory_space=pltpu.VMEM)
     hbm = pl.BlockSpec(memory_space=pltpu.HBM)
     dma = pltpu.SemaphoreType.DMA
     shape = jax.ShapeDtypeStruct
-    slab = (groups, 2 * capacity, LANE)
+    slab = (2, groups, capacity, LANE)
     scratch = [
         pltpu.VMEM((2, tokens), jnp.int32),
         pltpu.VMEM((2, tokens), F32),
@@ -607,9 +629,10 @@
         pltpu.VMEM((groups, DK, LANE), BF),
         pltpu.VMEM((DK, LANE), F32),
         dma((3,)), dma((11,)),
-        dma((firsts,)), dma((firsts,)),
+        dma((firsts, 2)), dma((firsts, 2)),
         dma((2, 2, 2)), dma((2, 2, 2)),
         dma((chips,)), dma((chips,)),
+        dma((2, 2)), dma((2, 2)),
         dma((chips,)), dma((chips,)),
         dma((2,)), dma((2,)),
         dma((chips,)), dma((chips,)),

time: 71.7 us -> 68.8 us (0.960)
  Pallas kernels: 70.9 us -> 68 us
    pallas_call x1, Pallas kernels: 68.6 us -> 65.7 us  [on_device(): pl.pallas_call(functools.partial(main_kernel, groups=groups, lanes=lanes,...]
where the time goes in v4:
time: 68.8 us; the launch traced here: 68.7 us
  Pallas kernels  68 us (99%)
    pallas_call x1, Pallas kernels, on_device(): pl.pallas_call(functools.partial(main_kernel, groups=groups, lanes=lanes,...  65.7 us
    pallas_call x1, Pallas kernels, on_device(): pl.pallas_call(store_kernel, name='store_results', out_shape=tuple((shape...  2.28 us

profile of v4, /device:TPU:1, one launch (start us, length us, event | category | flops | bytes accessed | tf_op | source)
XLA Modules:
  0.0 68.7 jit_solution(18272817577991506346)
XLA Ops:
  0.6 65.7 %experts_and_attention.1 = (bf16[2048,384]{1,0:T(8,128)(2,1)S(1)}, bf16[2048,384]{1,0:T(8,128)(2,1)S(1)}, bf16[384,2048]{1,0:T(8,128)(2,1)S(1)}, f32[128,128]{1,...) custom-call(s32[2,128]{1,0:T(2,128)} %bitcast.11, ...), custom_call_target="tpu_custom_call" | custom-call | tf_op jit(solution)/shard_map/experts_and_attention/pallas_call | solution.py:656
  66.4 2.3 %store_results.1 = (bf16[1,2048,384]{2,1,0:T(8,128)(2,1)}, bf16[1,2048,384]{2,1,0:T(8,128)(2,1)}, bf16[1,384,2048]{2,1,0:T(8,128)(2,1)}, f32[128,128]{1,0:T(8,12...) custom-call(bf16[2048,384]{1,0:T(8,128)(2,1)S(1)} %get-tuple-element.24.re, ...), custom_call_target="tpu_custom_call" | custom-call | tf_op jit(solution)/shard_map/store_results/pallas_call | solution.py:670

commit v5 on v4

--- a/solution.py
+++ b/solution.py
@@ -479,14 +479,12 @@
         waited(grad_in.at[t, pl.ds(0, half_rows)], opp_r.at[side])
     to_pair(chips // 2, t)
     to_owner(t)
+    mix = jnp.zeros((tokens, LANE), F32)
     for rel in [0, *order, chips // 2]:
-        t = wrapped(chips - rel if rel else 0) * 2 + other
-        waited(grad_in.at[t], fwd_r.at[rel])
-
-    mix = jnp.zeros((tokens, LANE), F32)
-    for zz in range(chips):
+        zz = wrapped(chips - rel if rel else 0)
+        waited(grad_in.at[zz * 2 + other], fwd_r.at[rel])
         pair = jnp.concatenate([grad_in[2 * zz], grad_in[2 * zz + 1]], axis=1)
-        mix += mm(pair, proj_ref[:, 2 * zz * LANE : 2 * (zz + 1) * LANE], NT)
+        mix += mm(pair, proj_ref[:, depth_of(zz)], NT)
 
     scale = DK ** (-0.5)
     grown = jnp.exp(cum)
@@ -528,6 +526,16 @@
         waited(all_in.at[pl.ds(0, groups - 1)], pj_r)
         to_tp(all_in, all_in, mate_s, mate_r, z, other)
 
+    @pl.when(jnp.logical_not(mate))
+    def _():
+        waited(all_in, mate_r)
+
+    waited(all_saved.at[pl.ds(0, groups - 1)], save_r)
+    depth = groups * tokens
+    gproj_ref[...] = mm(
+        all_in[...].reshape(depth, LANE), all_saved[...].reshape(depth, LANE), TN
+    )
+
     after[...] = jnp.zeros_like(after)
     for s in range(1, groups):
         @pl.when(s > sp)
@@ -548,15 +556,6 @@
     gk_ref[...] = dk.astype(BF)
     gv_ref[...] = dv.astype(BF)
 
-    @pl.when(jnp.logical_not(mate))
-    def _():
-        waited(all_in, mate_r)
-
-    waited(all_saved.at[pl.ds(0, groups - 1)], save_r)
-    depth = groups * tokens
-    gproj_ref[...] = mm(
-        all_in[...].reshape(depth, LANE), all_saved[...].reshape(depth, LANE), TN
-    )
     drain(6)
 
 
@@ -564,10 +563,18 @@
     count = (len(refs) - 1) // 2
     sems = refs[-1]
     copies = []
-    for n, (src, dst) in enumerate(zip(refs[:count], refs[count : 2 * count])):
-        copy = pltpu.make_async_copy(src, dst.at[0] if len(dst.shape) > 2 else dst, sems.at[n])
+    for src, dst in zip(refs[:count], refs[count : 2 * count]):
+        if len(dst.shape) > 2:
+            rows = src.shape[0] // 4
+            pairs = [
+                (src.at[pl.ds(k * rows, rows)], dst.at[0, pl.ds(k * rows, rows)]) for k in range(4)
+            ]
+        else:
+            pairs = [(src, dst)]
+        for part, place in pairs:
+            copies.append(pltpu.make_async_copy(part, place, sems.at[len(copies)]))
+    for copy in copies:
         copy.start()
-        copies.append(copy)
     for copy in copies:
         copy.wait()
 
@@ -675,7 +682,7 @@
         ),
         in_specs=[vmem] * 8,
         out_specs=(hbm,) * 8,
-        scratch_shapes=[dma((8,))],
+        scratch_shapes=[dma((17,))],
         compiler_params=pltpu.CompilerParams(vmem_limit_bytes=1024 * 1024),
     )(*(pltpu.with_memory_space_constraint(r, pltpu.VMEM) for r in results))
     gg, gu, gw, gp, gq, gk, gv, gd = results

time: 68.8 us -> 69 us (level)
  no operation moved by 1% of the time
where the time goes in v5:
time: 69 us; the launch traced here: 68.9 us
  Pallas kernels  68.2 us (99%)
    pallas_call x1, Pallas kernels, on_device(): pl.pallas_call(functools.partial(main_kernel, groups=groups, lanes=lanes,...  65.9 us
    pallas_call x1, Pallas kernels, on_device(): pl.pallas_call(store_kernel, name='store_results', out_shape=tuple((shape...  2.35 us

profile of v5, /device:TPU:1, one launch (start us, length us, event | category | flops | bytes accessed | tf_op | source)
XLA Modules:
  0.0 68.9 jit_solution(8760499845827241335)
XLA Ops:
  0.6 65.9 %experts_and_attention.1 = (bf16[2048,384]{1,0:T(8,128)(2,1)S(1)}, bf16[2048,384]{1,0:T(8,128)(2,1)S(1)}, bf16[384,2048]{1,0:T(8,128)(2,1)S(1)}, f32[128,128]{1,...) custom-call(s32[2,128]{1,0:T(2,128)} %bitcast.11, ...), custom_call_target="tpu_custom_call" | custom-call | tf_op jit(solution)/shard_map/experts_and_attention/pallas_call | solution.py:663
  66.5 2.3 %store_results.1 = (bf16[1,2048,384]{2,1,0:T(8,128)(2,1)}, bf16[1,2048,384]{2,1,0:T(8,128)(2,1)}, bf16[1,384,2048]{2,1,0:T(8,128)(2,1)}, f32[128,128]{1,0:T(8,12...) custom-call(bf16[2048,384]{1,0:T(8,128)(2,1)S(1)} %get-tuple-element.24.re, ...), custom_call_target="tpu_custom_call" | custom-call | tf_op jit(solution)/shard_map/store_results/pallas_call | solution.py:677
